TPU v7x, 32 devices: a whole 2x2x4 slice. The times are simulated.
32 devices in a mesh: sp: 8 (over z, x), tp: 4 (over y, core).
Axes of the slice: x: 2, y: 2, z: 4, core: 2. Of those that a mesh axis runs over, the one named last changes fastest.
Arguments:
- tokens: bfloat16 [4096, 2048], P('sp', 'tp'), may hold values from -400 to 400
- lru_in: bfloat16 [2048, 1024], P(None, 'tp'), may hold values from -0.125 to 0.125
- lru_gate_in: bfloat16 [2048, 1024], P(None, 'tp'), may hold values from -0.125 to 0.125
- query_w: bfloat16 [2048, 1024], P(None, 'tp'), may hold values from -1 to 1
- key_w: bfloat16 [2048, 1024], P(None, 'tp'), may hold values from -10 to 10
- value_w: bfloat16 [2048, 1024], P(None, 'tp'), may hold values from -0.125 to 0.125
- conv_weight: bfloat16 [4, 1024], replicated, may hold values from -3 to 3
- recur_gate_w: bfloat16 [16, 64, 64], replicated, may hold values from -0.75 to 0.75
- input_gate_w: bfloat16 [16, 64, 64], replicated, may hold values from -0.75 to 0.75
- rate_param: float32 [1024], replicated, may hold values from 0 to 16
- decay_extra: float32 [4096, 1024], P('sp', 'tp'), may hold values from -2 to 0
- forget_cum: float32 [4096, 8], P('sp', 'tp'), may hold values from -386 to 0, as said below
- out_lru: bfloat16 [1024, 2048], P('tp'), may hold values from -0.1875 to 0.1875
- out_fox: bfloat16 [1024, 2048], P('tp'), may hold values from -0.1875 to 0.1875
Outputs:
- mixed_out: bfloat16 [4096, 2048], P('sp', 'tp')
Inputs may be any that keep to these rules, and one draw needn't show every extreme that they name: `forget_cum`: non-increasing along positions in every head.
All inputs are finite; a program needn't handle non-finite values.
Results may differ from a plain program's by a relative error of at most 0.014.
Values may be sent and summed in bfloat16 or wider, within the bound.
A program may use at most 64 MiB of HBM per device.

v0:
```python
import functools

import jax
import jax.numpy as jnp
from jax import lax
from jax.experimental import pallas as pl
from jax.experimental.pallas import tpu as pltpu
from jax.sharding import PartitionSpec as P

HEAD_DIM = 128
decay_sharpness = 8.0
epsilon_norm = 1e-06
MESH = pl.DeviceIdType.MESH
F32 = jnp.float32
BF16 = jnp.bfloat16


def one_minus_exp(w):
    u = -w
    series = 1.0 - u / 9.0
    for n in range(8, 1, -1):
        series = 1.0 - u / n * series
    return jnp.where(u < 0.5, u * series, 1.0 - jnp.exp(w))


def remote(src, dst, send_sem, recv_sem, device):
    return pltpu.make_async_remote_copy(
        src_ref=src,
        dst_ref=dst,
        send_sem=send_sem,
        recv_sem=recv_sem,
        device_id=device,
        device_id_type=MESH,
    )


def kernel(
    SP,
    TP,
    X,
    tokens,
    lru_in,
    gate_in,
    query_w,
    key_w,
    value_w,
    conv_w,
    rg_w,
    ig_w,
    rate,
    decay_extra,
    forget,
    out_lru,
    out_fox,
    out,
    tok_buf,
    w_buf,
    acc,
    sq,
    lru_ref,
    halo,
    pad,
    bd_r,
    bd_i,
    gate_ref,
    q_ref,
    decay_buf,
    prefix_ref,
    local_ref,
    ends,
    incoming,
    kv_buf,
    cum_buf,
    cum_pad,
    wide,
    fcol,
    m_ref,
    l_ref,
    o_ref,
    q_far,
    m_far,
    l_far,
    o_far,
    part_out,
    stat_out,
    part_in,
    stat_in,
    wl_buf,
    wf_buf,
    br_lru,
    br_fox,
    oacc,
    load_sem,
    tsend,
    tfwd,
    trecv,
    hsend,
    hrecv,
    esend,
    erecv,
    zsend,
    xsend,
    kvrecv,
    wsend,
    wrecv,
    lsend,
    lrecv,
    fsend,
    ffwd,
    frecv,
    lfwd,
    qsend,
    qrecv,
    osend,
    orecv,
):
    rows, dcols = tokens.shape
    D, lw = lru_in.shape
    fw = query_w.shape[1]
    H = fw // HEAD_DIM
    oc = out.shape[1]
    Y = TP // 2
    Z = SP // X
    CH = tsend.shape[1]
    rc = rows // CH
    sp = lax.axis_index("sp")
    tp = lax.axis_index("tp")
    z = lax.div(sp, X)
    x = lax.rem(sp, X)
    partner = tp + 1 - 2 * lax.rem(tp, 2)
    far = [lax.rem(tp + 2 * k, TP) for k in range(Y)]
    pfar = [lax.rem(partner + 2 * k, TP) for k in range(Y)]
    offs = [0, lw, lw + fw, lw + 2 * fw, 2 * lw + 2 * fw, 2 * lw + 3 * fw]

    barrier = pltpu.get_barrier_semaphore()
    for k in range(1, SP):
        pl.semaphore_signal(
            barrier, inc=1, device_id={"sp": lax.rem(sp + k, SP)}, device_id_type=MESH
        )
    for k in range(1, TP):
        pl.semaphore_signal(
            barrier, inc=1, device_id={"tp": lax.rem(tp + k, TP)}, device_id_type=MESH
        )
    loads = []
    for i, w in enumerate((lru_in, key_w, value_w, gate_in, query_w)):
        c = pltpu.make_async_copy(w, w_buf.at[:, offs[i] : offs[i + 1]], load_sem.at[i])
        c.start()
        loads.append(c)
    mine = pl.ds(pl.multiple_of(tp * oc, 128), oc)
    own_loads = [
        pltpu.make_async_copy(decay_extra, decay_buf, load_sem.at[5]),
        pltpu.make_async_copy(out_lru.at[:, mine], wl_buf.at[tp], load_sem.at[6]),
        pltpu.make_async_copy(out_fox.at[:, mine], wf_buf.at[tp], load_sem.at[7]),
    ]
    for c in own_loads:
        c.start()
    pl.semaphore_wait(barrier, SP - 1 + TP - 1)

    pending = []

    def chunk(c):
        return pl.ds(c * rc, rc)

    for c in range(CH):
        for k in range(1, Y):
            s = remote(
                tokens.at[chunk(c)],
                tok_buf.at[tp, chunk(c)],
                tsend.at[k, c],
                trecv.at[tp, c],
                {"tp": far[k]},
            )
            s.start()
            pending.append(s)
    for c in range(CH):
        s = remote(
            tokens.at[chunk(c)],
            tok_buf.at[tp, chunk(c)],
            tsend.at[0, c],
            trecv.at[tp, c],
            {"tp": partner},
        )
        s.start()
        pending.append(s)

    bw = rg_w.shape[1]
    nb = lw // bw
    bd_r[...] = jnp.zeros_like(bd_r)
    bd_i[...] = jnp.zeros_like(bd_i)
    for n in range(nb):
        sl = pl.ds(n * bw, bw)
        bd_r[sl, sl] = rg_w[tp * nb + n]
        bd_i[sl, sl] = ig_w[tp * nb + n]
    cum_pad[...] = jnp.zeros_like(cum_pad)
    wide[...] = jnp.zeros_like(wide)
    wide[0:H, :] = forget[...]
    fcol[...] = wide[...].T
    cum_buf[sp] = wide[0:8, :]

    for c in loads:
        c.wait()

    def project(val, src, r, first=False):
        w_rows = pl.ds(pl.multiple_of(src * dcols, dcols), dcols)
        v32 = val.astype(F32)
        part = jnp.sum(v32 * v32, axis=1, keepdims=True)
        dot = jnp.dot(val, w_buf[w_rows, :], preferred_element_type=F32)
        if first:
            sq[r, :] = part
            acc[r, :] = dot
        else:
            sq[r, :] += part
            acc[r, :] += dot

    def tok_wait(src, c):
        ref = tok_buf.at[src, chunk(c)]
        remote(ref, ref, tsend.at[0, c], trecv.at[src, c], {"tp": partner}).wait_recv()

    for c in range(CH):
        project(tokens[chunk(c), :], tp, chunk(c), True)
    for c in range(CH):
        tok_wait(partner, c)
        project(tok_buf[partner, chunk(c), :], partner, chunk(c))
    for c in range(CH):
        for k in range(1, Y):
            tok_wait(far[k], c)
            ref = tok_buf.at[far[k], chunk(c)]
            s = remote(ref, ref, tfwd.at[k, c], trecv.at[far[k], c], {"tp": partner})
            s.start()
            pending.append(s)
            project(tok_buf[far[k], chunk(c), :], far[k], chunk(c))
        for k in range(1, Y):
            tok_wait(pfar[k], c)
            project(tok_buf[pfar[k], chunk(c), :], pfar[k], chunk(c))

    row_scale = lax.rsqrt(sq[...] / D + epsilon_norm)

    def scaled(i, n=1):
        return (acc[:, offs[i] : offs[i + n]] * row_scale).astype(BF16)

    lru_ref[...] = scaled(0)
    hb = halo.shape[0]
    halo_copy = remote(
        lru_ref.at[pl.ds(rows - hb, hb)],
        halo,
        hsend.at[0],
        hrecv.at[0],
        {"sp": lax.rem(sp + 1, SP)},
    )

    @pl.when(sp < SP - 1)
    def _():
        halo_copy.start()

    kv_buf[sp] = scaled(1, 2)

    paired = Z in (3, 4)
    helper = jnp.logical_and(z <= Z - 3, paired)
    helped = jnp.logical_and(z >= 2, paired)

    def block_copies(j, a, send_sem, device):
        return (
            remote(kv_buf.at[j], kv_buf.at[j], send_sem.at[a, 0], kvrecv.at[j, 0], device),
            remote(cum_buf.at[j], cum_buf.at[j], send_sem.at[a, 1], kvrecv.at[j, 1], device),
        )

    def z_copies(dz):
        j = (z - dz) * X + x
        return block_copies(j, dz, zsend, {"sp": lax.rem(sp + X, SP)})

    def x_copies(dz, dx):
        j = (z - dz) * X + x
        xo = lax.rem(x + dx, X)
        return block_copies(j, dz, xsend.at[dx - 1], {"sp": z * X + xo})

    def for_sends(dz, own, act):
        if own or not paired:

            @pl.when(z < Z - 1)
            def _():
                for c in z_copies(dz):
                    act(c)

        for dx in range(1, X):
            if own:

                @pl.when(jnp.logical_or(lax.rem(x + dx, X) > x, helper))
                def _():
                    for c in x_copies(dz, dx):
                        act(c)
            else:
                for c in x_copies(dz, dx):
                    act(c)

    def kv_wait(j):
        for c in block_copies(j, 0, zsend, {"sp": lax.rem(sp + X, SP)}):
            c.wait_recv()

    for_sends(0, True, lambda c: c.start())

    q_ref[...] = scaled(4)
    q_copy = remote(
        q_ref, q_far, qsend.at[0], qrecv.at[0], {"sp": lax.rem(sp + SP - 2 * X, SP)}
    )

    @pl.when(helped)
    def _():
        q_copy.start()

    for i, (w, buf) in enumerate(((out_lru, wl_buf), (out_fox, wf_buf))):
        for k in range(1, TP):
            t = lax.rem(tp + k, TP)
            cols = pl.ds(pl.multiple_of(t * oc, 128), oc)
            s = remote(w.at[:, cols], buf.at[tp], wsend.at[i, k], wrecv.at[i, tp], {"tp": t})
            s.start()
            pending.append(s)

    gate_ref[...] = scaled(3)

    @pl.when(sp == 0)
    def _():
        pad[0:8, :] = jnp.zeros((8, lw), F32)

    @pl.when(sp > 0)
    def _():
        halo_copy.wait_recv()
        pad[0:8, :] = halo[...].astype(F32)[hb - 8 : hb, :]

    pad[8 : 8 + rows, :] = lru_ref[...].astype(F32)
    chans = pl.ds(pl.multiple_of(tp * lw, 128), lw)
    taps = conv_w.shape[0]
    taps_f32 = conv_w[:, chans].astype(F32)
    conv = jnp.zeros((rows, lw), F32)
    for j in range(taps):
        conv = conv + taps_f32[j : j + 1, :] * pad[8 - (taps - 1) + j : 8 - (taps - 1) + j + rows, :]
    conv_b = conv.astype(BF16)

    def sigmoid(v):
        return 1.0 / (1.0 + jnp.exp(-v))

    recur_gate = sigmoid(jnp.dot(conv_b, bd_r[...], preferred_element_type=F32))
    input_gate = sigmoid(jnp.dot(conv_b, bd_i[...], preferred_element_type=F32))
    own_rate = rate[:, chans]
    softplus = jnp.maximum(-own_rate, 0.0) + jnp.log1p(jnp.exp(-jnp.abs(own_rate)))
    for c in own_loads:
        c.wait()
    log_decay = -decay_sharpness * softplus * recur_gate + decay_buf[...]
    prefix_ref[...] = jnp.exp(log_decay)
    local_ref[...] = jnp.sqrt(one_minus_exp(2.0 * log_decay)) * input_gate * conv_b.astype(F32)
    row_id = lax.broadcasted_iota(jnp.int32, (rows, lw), 0)
    step = 1
    while step < rows:
        a = prefix_ref[...]
        b = local_ref[...]
        keep = row_id >= step
        a_prev = jnp.where(keep, pltpu.roll(a, step, 0), 1.0)
        b_prev = jnp.where(keep, pltpu.roll(b, step, 0), 0.0)
        local_ref[...] = b + a * b_prev
        prefix_ref[...] = a * a_prev
        step *= 2
    ends[sp, 0:1, :] = prefix_ref[rows - 1 : rows, :]
    ends[sp, 1:2, :] = local_ref[rows - 1 : rows, :]

    def end_copy(k):
        return remote(
            ends.at[sp], ends.at[sp], esend.at[k], erecv.at[sp], {"sp": lax.rem(sp + k, SP)}
        )

    for k in range(1, SP):

        @pl.when(sp + k < SP)
        def _():
            end_copy(k).start()

    score_scale = HEAD_DIM ** (-0.5)
    qc = rows // 2

    def attend(j, diagonal, far_first=None):
        other = far_first is not None
        first = diagonal or far_first
        qs, ms, ls, os = (q_far, m_far, l_far, o_far) if other else (q_ref, m_ref, l_ref, o_ref)

        def some(i, carry):
            r = pl.ds(pl.multiple_of(i * qc, qc), qc)
            for h in range(H):
                hs = slice(h * HEAD_DIM, (h + 1) * HEAD_DIM)
                vs = slice(fw + h * HEAD_DIM, fw + (h + 1) * HEAD_DIM)
                s = lax.dot_general(
                    qs[r, hs],
                    kv_buf[j, :, hs],
                    (((1,), (1,)), ((), ())),
                    preferred_element_type=F32,
                )
                s = s * score_scale
                if not other:
                    s = s + fcol[r, h : h + 1]
                s = s - cum_buf[j, h : h + 1, :]
                if diagonal:
                    causal = (
                        lax.broadcasted_iota(jnp.int32, (qc, rows), 0) + i * qc
                        >= lax.broadcasted_iota(jnp.int32, (qc, rows), 1)
                    )
                    s = jnp.where(causal, s, -1e30)
                top = jnp.max(s, axis=1, keepdims=True)
                if first:
                    p = jnp.exp(s - top)
                    ms[h, r, :] = top
                    ls[h, r, :] = jnp.sum(p, axis=1, keepdims=True)
                    os[h, r, :] = jnp.dot(
                        p.astype(BF16), kv_buf[j, :, vs], preferred_element_type=F32
                    )
                else:
                    old = ms[h, r, :]
                    new = jnp.maximum(old, top)
                    p = jnp.exp(s - new)
                    fade = jnp.exp(old - new)
                    ms[h, r, :] = new
                    ls[h, r, :] = ls[h, r, :] * fade + jnp.sum(p, axis=1, keepdims=True)
                    os[h, r, :] = os[h, r, :] * fade + jnp.dot(
                        p.astype(BF16), kv_buf[j, :, vs], preferred_element_type=F32
                    )
            return carry

        lax.fori_loop(0, rows // qc, some, 0)

    attend(sp, True)

    def row_blocks(dz):
        for dx in range(1, X):
            xo = lax.rem(x + dx, X)

            @pl.when(jnp.logical_or(dz > 0, xo < x))
            def _():
                j = (z - dz) * X + xo
                kv_wait(j)
                attend(j, False)

    def finish_lru():
        incoming[...] = jnp.zeros_like(incoming)
        for j in range(SP - 1):

            @pl.when(j < sp)
            def _():
                remote(
                    ends.at[j], ends.at[j], esend.at[0], erecv.at[j], {"sp": lax.rem(sp + 1, SP)}
                ).wait_recv()
                incoming[...] = ends[j, 0:1, :] * incoming[...] + ends[j, 1:2, :]

        states = local_ref[...] + prefix_ref[...] * incoming[...]
        g = gate_ref[...].astype(F32)
        gelu = 0.5 * g * (1.0 + jnp.tanh(0.7978845608028654 * (g + 0.044715 * (g * g * g))))
        br_lru[tp] = (states * gelu).astype(BF16)
        for k in range(Y - 1, -1, -1):
            lru_copy(k).start()

    def lru_copy(k):
        to = far[k] if k else partner
        return remote(br_lru.at[tp], br_lru.at[tp], lsend.at[k], lrecv.at[tp], {"tp": to})

    lru_step = min(2, Z - 1)
    if Z == 1:
        finish_lru()

    def hop(dz, carry):
        @pl.when(dz <= z)
        def _():
            j = (z - dz) * X + x
            kv_wait(j)
            for_sends(dz, False, lambda c: c.start())
            row_blocks(dz - 1)
            attend(j, False)

        @pl.when(dz == lru_step)
        def _():
            finish_lru()

        return carry

    up = {"sp": lax.rem(sp + 2 * X, SP)}
    part_copies = (
        remote(part_out, part_in, osend.at[0], orecv.at[0], up),
        remote(stat_out, stat_in, osend.at[1], orecv.at[1], up),
    )

    def send_partial():
        for h in range(H):
            part_out[:, h * HEAD_DIM : (h + 1) * HEAD_DIM] = o_far[h].astype(BF16)
            cum_pad[:, h : h + 1] = m_far[h]
            cum_pad[:, H + h : H + h + 1] = l_far[h]
        stat_out[...] = cum_pad[...].T[0:8, :]
        for c in part_copies:
            c.start()

    if paired:
        below = (z - 1) * X

        @pl.when(helper)
        def _():
            q_copy.wait_recv()
            attend(sp, False, True)

        @pl.when(z >= 1)
        def _():
            kv_wait(below + x)
            for_sends(1, False, lambda c: c.start())

        for dx in range(1, X):
            xo = lax.rem(x + dx, X)

            @pl.when(jnp.logical_or(xo < x, helper))
            def _():
                kv_wait(z * X + xo)

            @pl.when(helper)
            def _():
                attend(z * X + xo, False, False)

        @pl.when(jnp.logical_and(helper, z == 0))
        def _():
            send_partial()

        for dx in range(1, X):
            xo = lax.rem(x + dx, X)

            @pl.when(xo < x)
            def _():
                attend(z * X + xo, False)

        finish_lru()

        @pl.when(jnp.logical_and(helper, z >= 1))
        def _():
            attend(below + x, False, False)

        @pl.when(z >= 1)
        def _():
            attend(below + x, False)
            for dx in range(1, X):
                j = below + lax.rem(x + dx, X)
                kv_wait(j)

                @pl.when(helper)
                def _():
                    attend(j, False, False)

            @pl.when(helper)
            def _():
                send_partial()

            for dx in range(1, X):
                attend(below + lax.rem(x + dx, X), False)

    else:
        lax.fori_loop(1, Z, hop, 0)

    def lru_wait(t):
        remote(br_lru.at[t], br_lru.at[t], lsend.at[0], lrecv.at[t], {"tp": partner}).wait_recv()

    def lru_dot(t):
        return jnp.dot(br_lru[t], wl_buf[t], preferred_element_type=F32)

    oacc[...] = lru_dot(tp)
    for k in range(1, TP):
        t = lax.rem(tp + k, TP)
        for i, buf in enumerate((wl_buf, wf_buf)):
            remote(buf.at[t], buf.at[t], wsend.at[i, k], wrecv.at[i, t], {"tp": t}).wait_recv()
    for k in range(1, Y):
        lru_wait(far[k])
        ref = br_lru.at[far[k]]
        s = remote(ref, ref, lfwd.at[k], lrecv.at[far[k]], {"tp": partner})
        s.start()
        pending.append(s)
    lru_wait(partner)
    oacc[...] += lru_dot(partner)
    for k in range(1, Y):
        oacc[...] += lru_dot(far[k])
        lru_wait(pfar[k])
        oacc[...] += lru_dot(pfar[k])

    if paired:

        @pl.when(helped)
        def _():
            for c in part_copies:
                c.wait_recv()
            wide[0:8, :] = stat_in[...]
            stats = wide[...].T
            for h in range(H):
                m_in = stats[:, h : h + 1] + fcol[:, h : h + 1]
                l_in = stats[:, H + h : H + h + 1]
                part = part_in[:, h * HEAD_DIM : (h + 1) * HEAD_DIM].astype(F32)
                new = jnp.maximum(m_ref[h], m_in)
                fade = jnp.exp(m_ref[h] - new)
                grow = jnp.exp(m_in - new)
                l_ref[h] = l_ref[h] * fade + l_in * grow
                o_ref[h] = o_ref[h] * fade + part * grow

    else:
        row_blocks(z)

    for c in range(CH):
        r = chunk(c)
        for h in range(H):
            br_fox[tp, r, h * HEAD_DIM : (h + 1) * HEAD_DIM] = (
                o_ref[h, r, :] / l_ref[h, r, :]
            ).astype(BF16)
        ref = br_fox.at[tp, r]
        for k in list(range(1, Y)) + [0]:
            to = far[k] if k else partner
            s = remote(ref, ref, fsend.at[k, c], frecv.at[tp, c], {"tp": to})
            s.start()
            pending.append(s)

    def fox_wait(src, c):
        ref = br_fox.at[src, chunk(c)]
        remote(ref, ref, fsend.at[0, c], frecv.at[src, c], {"tp": partner}).wait_recv()

    def fox_dot(src, r):
        return jnp.dot(br_fox[src, r, :], wf_buf[src], preferred_element_type=F32)

    for c in range(CH):
        fox_wait(partner, c)
        oacc[chunk(c), :] += fox_dot(tp, chunk(c)) + fox_dot(partner, chunk(c))
    for c in range(CH):
        r = chunk(c)
        for k in range(1, Y):
            fox_wait(far[k], c)
            ref = br_fox.at[far[k], r]
            s = remote(ref, ref, ffwd.at[k, c], frecv.at[far[k], c], {"tp": partner})
            s.start()
            pending.append(s)
            oacc[r, :] += fox_dot(far[k], r)
        for k in range(1, Y):
            fox_wait(pfar[k], c)
            oacc[r, :] += fox_dot(pfar[k], r)
        out[r, :] = oacc[r, :].astype(out.dtype)

    for s in pending:
        s.wait_send()
    for k in range(Y):
        lru_copy(k).wait_send()

    @pl.when(helped)
    def _():
        q_copy.wait_send()

    @pl.when(helper)
    def _():
        for c in part_copies:
            c.wait_send()

    @pl.when(sp < SP - 1)
    def _():
        halo_copy.wait_send()

    for k in range(1, SP):

        @pl.when(sp + k < SP)
        def _():
            end_copy(k).wait_send()

    for_sends(0, True, lambda c: c.wait_send())

    def drain(dz, carry):
        @pl.when(dz <= z)
        def _():
            for_sends(dz, False, lambda c: c.wait_send())

        return carry

    if paired:

        @pl.when(z >= 1)
        def _():
            for_sends(1, False, lambda c: c.wait_send())

    else:
        lax.fori_loop(1, Z, drain, 0)


def shards(SP, TP, X, *args):
    tokens, lru_in, gate_in, query_w = args[:4]
    (conv_weight, rg_w, ig_w, rate, decay_extra, forget, out_lru, out_fox) = args[6:]
    rows, dcols = tokens.shape
    D, lw = lru_in.shape
    fw = query_w.shape[1]
    oc = out_lru.shape[1] // TP
    tot = 2 * lw + 3 * fw
    H = fw // HEAD_DIM
    Y = TP // 2
    Z = SP // X
    CH = 4
    vm = pl.BlockSpec(memory_space=pltpu.VMEM)
    hbm = pl.BlockSpec(memory_space=pl.ANY)
    dma = pltpu.SemaphoreType.DMA
    V = pltpu.VMEM
    scratch = [
        V((TP, rows, dcols), BF16),
        V((D, tot), BF16),
        V((rows, tot), F32),
        V((rows, 1), F32),
        V((rows, lw), BF16),
        V((16, lw), BF16),
        V((rows + 8, lw), F32),
        V((lw, lw), BF16),
        V((lw, lw), BF16),
        V((rows, lw), BF16),
        V((rows, fw), BF16),
        V((rows, lw), F32),
        V((rows, lw), F32),
        V((rows, lw), F32),
        V((SP, 8, lw), F32),
        V((1, lw), F32),
        V((SP, rows, 2 * fw), BF16),
        V((SP, 8, rows), F32),
        V((rows, 128), F32),
        V((128, rows), F32),
        V((rows, 128), F32),
        V((H, rows, 1), F32),
        V((H, rows, 1), F32),
        V((H, rows, HEAD_DIM), F32),
        V((rows, fw), BF16),
        V((H, rows, 1), F32),
        V((H, rows, 1), F32),
        V((H, rows, HEAD_DIM), F32),
        V((rows, fw), BF16),
        V((8, rows), F32),
        V((rows, fw), BF16),
        V((8, rows), F32),
        V((TP, lw, oc), BF16),
        V((TP, fw, oc), BF16),
        V((TP, rows, lw), BF16),
        V((TP, rows, fw), BF16),
        V((rows, oc), F32),
        dma((8,)),
        dma((Y, CH)),
        dma((Y, CH)),
        dma((TP, CH)),
        dma((1,)),
        dma((1,)),
        dma((SP,)),
        dma((SP,)),
        dma((Z, 2)),
        dma((max(X - 1, 1), Z, 2)),
        dma((SP, 2)),
        dma((2, TP)),
        dma((2, TP)),
        dma((TP,)),
        dma((TP,)),
        dma((Y, CH)),
        dma((Y, CH)),
        dma((TP, CH)),
        dma((Y,)),
        dma((1,)),
        dma((1,)),
        dma((2,)),
        dma((2,)),
    ]
    return pl.pallas_call(
        functools.partial(kernel, SP, TP, X),
        out_shape=jax.ShapeDtypeStruct((rows, oc), BF16),
        in_specs=[vm] + [hbm] * 5 + [vm] * 4 + [hbm, vm, hbm, hbm],
        out_specs=vm,
        scratch_shapes=scratch,
        compiler_params=pltpu.CompilerParams(
            collective_id=0, has_side_effects=True, vmem_limit_bytes=60 * 1024 * 1024
        ),
    )(*args[:9], rate.reshape(1, -1), decay_extra, forget.T, out_lru, out_fox)


def columns_of(mesh):
    SP = mesh.shape["sp"]
    try:
        X = len({d.coords[0] for d in mesh.devices.flat})
    except AttributeError:
        X = 2
    return X if SP % X == 0 else 1


def solution(mesh):
    placed = (
        P("sp", "tp"),
        P(None, "tp"),
        P(None, "tp"),
        P(None, "tp"),
        P(None, "tp"),
        P(None, "tp"),
        P(),
        P(),
        P(),
        P(),
        P("sp", "tp"),
        P("sp", "tp"),
        P("tp", None),
        P("tp", None),
    )
    body = functools.partial(shards, mesh.shape["sp"], mesh.shape["tp"], columns_of(mesh))
    return jax.shard_map(
        body, mesh=mesh, in_specs=placed, out_specs=P("sp", "tp"), check_vma=False
    )
```

profile of v0, /device:TPU:25, one launch (start us, length us, event | category | flops | bytes accessed | tf_op | source)
XLA Modules:
  0.0 68.5 jit_solution(11853661333184795605)
XLA Ops:
  0.0 66.6 %shard_map.136 = bf16[512,512]{1,0:T(8,128)(2,1)} custom-call(bf16[512,512]{1,0:T(8,128)(2,1)} %tokens.1, bf16[2048,256]{1,0:T(8,128)(2,1)} %lru_in.1, bf16[2048,256]{1,0:T(8,128)(2,1)} %gate_in.1, bf16[2048,256]{1,0:T(8,128)(2,1)} %query_w.1, bf16[2048,256]{1,0:T(8,128)(2,1)} %key_w.1, bf16[2048,256]{1,0:T(8,128)(2,1)} %value_w.1, bf16[4,1024]{1,0:T(4,128)(2,1)} %conv_w.1, ...), custom_call_target="tpu_custom_call" | custom-call | tf_op jit(solution)/shard_map/pallas_call | solution.py:759
  66.6 1.9 %copy.16 = bf16[512,512]{1,0:T(8,128)(2,1)} copy(bf16[512,512]{1,0:T(8,128)(2,1)} %shard_map.136) | data formatting | bytes 1048576
where the time goes:
time: 68.7 us; the launch traced here: 68.5 us
  Pallas kernels  66.6 us (97%)
  local copies, waits for them, and re-layouts  1.87 us (3%)
    pallas_call x1, Pallas kernels, shards(): pl.pallas_call(functools.partial(kernel, SP, TP, X), out_shape=jax.ShapeD...  66.6 us
    unnamed x1, local copies, waits for them, and re-layouts  1.87 us

commit v1 on v0

--- a/solution.py
+++ b/solution.py
@@ -768,6 +768,830 @@
     )(*args[:9], rate.reshape(1, -1), decay_extra, forget.T, out_lru, out_fox)
 
 
+LOG2E = 1.4426950408889634
+
+
+def block_kernel(
+    SP,
+    TP,
+    X,
+    CH,
+    tokens,
+    lru_in,
+    gate_in,
+    query_w,
+    key_w,
+    value_w,
+    conv_w,
+    rg_w,
+    ig_w,
+    rate,
+    decay_extra,
+    forget,
+    out_lru,
+    out_fox,
+    out,
+    tok_buf,
+    w_buf,
+    acc,
+    sq,
+    lru_ref,
+    halo,
+    pad,
+    conv_v,
+    rg_v,
+    ig_v,
+    rate_v,
+    forget_v,
+    bd_r,
+    bd_i,
+    gate_ref,
+    q_ref,
+    decay_buf,
+    prefix_ref,
+    local_ref,
+    seg_a,
+    seg_b,
+    carry_ref,
+    ends,
+    kv_buf,
+    cum_buf,
+    m_ref,
+    o_ref,
+    q_far,
+    m_far,
+    o_far,
+    part_out,
+    stat_out,
+    part_in,
+    stat_in,
+    wl_buf,
+    wf_buf,
+    br_lru,
+    br_fox,
+    oacc,
+    obuf,
+    load_sem,
+    out_sem,
+    tsend,
+    tfwd,
+    trecv,
+    hsend,
+    hrecv,
+    esend,
+    erecv,
+    csend,
+    crecv,
+    zsend,
+    xsend,
+    zfwd,
+    xfwd,
+    kvrecv,
+    wsend,
+    wfwd,
+    wrecv,
+    lsend,
+    lrecv,
+    fsend,
+    ffwd,
+    frecv,
+    lfwd,
+    qsend,
+    qrecv,
+    osend,
+    orecv,
+):
+    rows, dcols = tokens.shape
+    D, lw = lru_in.shape
+    fw = query_w.shape[1]
+    H = fw // HEAD_DIM
+    oc = out.shape[1]
+    Z = SP // X
+    rc = rows // CH
+    half = rows // 2
+    wh = out_lru.shape[0] // X
+    sp = lax.axis_index("sp")
+    tp = lax.axis_index("tp")
+    z = lax.div(sp, X)
+    x = lax.rem(sp, X)
+    xo = 1 - x
+    y = lax.div(tp, 2)
+    partner = tp + 1 - 2 * lax.rem(tp, 2)
+    far = lax.rem(tp + 2, TP)
+    pfar = lax.rem(partner + 2, TP)
+    j_xo = z * X + xo
+    to_xo = {"sp": j_xo}
+    to_up = {"sp": lax.rem(sp + X, SP)}
+    j_b = lax.rem(sp + SP - X, SP)
+    j_bo = lax.rem(j_xo + SP - X, SP)
+    helper = z <= Z - 3
+    helped = z >= 2
+    not_top = z < Z - 1
+    above0 = z >= 1
+    order = list(range(CH - 1, -1, -1))
+    via_z = order[0::2]
+    via_x = order[1::2]
+    score_k = HEAD_DIM ** (-0.5) * LOG2E
+
+    def chunk(c):
+        return pl.ds(c * rc, rc)
+
+    barrier = pltpu.get_barrier_semaphore()
+    for k in range(1, SP):
+        pl.semaphore_signal(
+            barrier, inc=1, device_id={"sp": lax.rem(sp + k, SP)}, device_id_type=MESH
+        )
+    for k in range(1, TP):
+        pl.semaphore_signal(
+            barrier, inc=1, device_id={"tp": lax.rem(tp + k, TP)}, device_id_type=MESH
+        )
+
+    def load(i, src, dst):
+        c = pltpu.make_async_copy(src, dst, load_sem.at[i])
+        c.start()
+        return c
+
+    tok_load = load(0, tokens, tok_buf.at[tp])
+    cols = (0, fw, 2 * fw, 2 * fw + lw, 3 * fw + lw, 3 * fw + 2 * lw)
+    w_loads = [
+        load(1 + i, w, w_buf.at[:, cols[i] : cols[i + 1]])
+        for i, w in enumerate((key_w, value_w, lru_in, query_w, gate_in))
+    ]
+    mine = pl.ds(pl.multiple_of(tp * oc, 128), oc)
+    bw = rg_w.shape[1]
+    nb = lw // bw
+    gates = pl.ds(tp * nb, nb)
+    forget_load = load(6, forget, forget_v)
+    small_loads = [
+        load(7, conv_w, conv_v),
+        load(8, rg_w.at[gates], rg_v),
+        load(9, ig_w.at[gates], ig_v),
+        load(10, rate, rate_v),
+        load(11, decay_extra, decay_buf),
+    ]
+    own_loads = [
+        load(12, out_lru.at[:, mine], wl_buf.at[tp]),
+        load(13, out_fox.at[:, mine], wf_buf.at[tp]),
+    ]
+    tok_load.wait()
+    pl.semaphore_wait(barrier, SP - 1 + TP - 1)
+
+    pending = []
+
+    def send(src, dst, send_sem, recv_sem, device):
+        s = remote(src, dst, send_sem, recv_sem, device)
+        s.start()
+        pending.append(s)
+
+    for c in order:
+        ref = tok_buf.at[tp, chunk(c)]
+        send(ref, ref, tsend.at[1, c], trecv.at[tp, c], {"tp": far})
+        send(ref, ref, tsend.at[0, c], trecv.at[tp, c], {"tp": partner})
+
+    forget_load.wait()
+    cum_buf[sp] = jnp.zeros_like(cum_buf[sp])
+    cum_buf[sp, 0:H, :] = forget_v[...] * LOG2E
+    own_cum = cum_buf.at[sp]
+    send(own_cum, own_cum, csend.at[0], crecv.at[sp], to_xo)
+    cum_up = (
+        remote(own_cum, own_cum, csend.at[1], crecv.at[sp], to_up),
+        remote(own_cum, own_cum, csend.at[2], crecv.at[sp], {"sp": lax.rem(j_xo + X, SP)}),
+    )
+
+    @pl.when(not_top)
+    def _():
+        for c in cum_up:
+            c.start()
+
+    for c in small_loads:
+        c.wait()
+    bd_r[...] = jnp.zeros_like(bd_r)
+    bd_i[...] = jnp.zeros_like(bd_i)
+    for n in range(nb):
+        sl = pl.ds(n * bw, bw)
+        bd_r[sl, sl] = rg_v[n]
+        bd_i[sl, sl] = ig_v[n]
+    for c in w_loads:
+        c.wait()
+
+    def tok_wait(src, c):
+        ref = tok_buf.at[src, chunk(c)]
+        remote(ref, ref, tsend.at[0, c], trecv.at[src, c], {"tp": partner}).wait_recv()
+
+    def features(side, c):
+        first = 2 * side
+        return jnp.concatenate([tok_buf[first, chunk(c), :], tok_buf[first + 1, chunk(c), :]], axis=1)
+
+    def w_rows(side):
+        return pl.ds(pl.multiple_of(side * 2 * dcols, 2 * dcols), 2 * dcols)
+
+    def squares(v):
+        v32 = v.astype(F32)
+        return jnp.sum(v32 * v32, axis=1, keepdims=True)
+
+    def near_part(c, slot):
+        tok_wait(partner, c)
+        v = features(y, c)
+        sq[slot] = squares(v)
+        acc[slot] = jnp.dot(v, w_buf[w_rows(y), :], preferred_element_type=F32)
+
+    halo_copy = remote(
+        lru_ref.at[pl.ds(rows - halo.shape[0], halo.shape[0])],
+        halo,
+        hsend.at[0],
+        hrecv.at[0],
+        {"sp": lax.rem(sp + 1, SP)},
+    )
+
+    def kv_copy(j, c, send_sem, device):
+        ref = kv_buf.at[j, chunk(c)]
+        return remote(ref, ref, send_sem.at[c], kvrecv.at[j, c], device)
+
+    def kv_wait(j, c):
+        kv_copy(j, c, zsend, to_up).wait_recv()
+
+    def across(c):
+        return jnp.logical_or(x == 0, z <= (Z - 2 if c in via_z else Z - 3))
+
+    def from_across(c):
+        return jnp.logical_or(x == 1, z <= (Z - 2 if c in via_z else Z - 3))
+
+    def q_copy(c):
+        return remote(
+            q_ref.at[chunk(c)],
+            q_far.at[chunk(c)],
+            qsend.at[c],
+            qrecv.at[c],
+            {"sp": lax.rem(sp + SP - 2 * X, SP)},
+        )
+
+    def far_part(i, c, slot):
+        tok_wait(far, c)
+        ref = tok_buf.at[far, chunk(c)]
+        send(ref, ref, tfwd.at[c], trecv.at[far, c], {"tp": partner})
+        if i + 1 < CH:
+            near_part(order[i + 1], 1 - slot)
+        tok_wait(pfar, c)
+        v = features(1 - y, c)
+        row_scale = lax.rsqrt((sq[slot] + squares(v)) / D + epsilon_norm)
+
+        def part(a, b):
+            w = w_buf[w_rows(1 - y), cols[a] : cols[b]]
+            both = acc[slot, :, cols[a] : cols[b]] + jnp.dot(v, w, preferred_element_type=F32)
+            return (both * row_scale).astype(BF16)
+
+        kv_buf[sp, chunk(c), :] = part(0, 2)
+
+        @pl.when(across(c))
+        def _():
+            kv_copy(sp, c, xsend, to_xo).start()
+
+        @pl.when(not_top)
+        def _():
+            kv_copy(sp, c, zsend, to_up).start()
+
+        rest = part(2, 5)
+        lru_ref[chunk(c), :] = rest[:, 0:lw]
+        q_ref[chunk(c), :] = rest[:, lw : lw + fw]
+        gate_ref[chunk(c), :] = rest[:, lw + fw :]
+
+        @pl.when(helped)
+        def _():
+            q_copy(c).start()
+
+        if i == 0:
+
+            @pl.when(sp < SP - 1)
+            def _():
+                halo_copy.start()
+
+    def weight_copy(i, w, buf, t, k):
+        r = pl.ds(x * wh, wh)
+        c = pl.ds(pl.multiple_of(t * oc, 128), oc)
+        return remote(w.at[r, c], buf.at[tp, r], wsend.at[i, k], wrecv.at[i, tp, x], {"tp": t})
+
+    near_part(order[0], 0)
+    for i, c in enumerate(order):
+        far_part(i, c, i % 2)
+        if i == CH - 2:
+            for n, (w, buf) in enumerate(((out_lru, wl_buf), (out_fox, wf_buf))):
+                for k, t in enumerate((far, pfar)):
+                    s = weight_copy(n, w, buf, t, k)
+                    s.start()
+                    pending.append(s)
+            for n, (w, buf) in enumerate(((out_lru, wl_buf), (out_fox, wf_buf))):
+                c2 = pl.ds(pl.multiple_of(partner * oc, 128), oc)
+                for k in range(X):
+                    r = pl.ds(k * wh, wh)
+                    send(
+                        w.at[r, c2],
+                        buf.at[tp, r],
+                        wsend.at[n, 2 + k],
+                        wrecv.at[n, tp, k],
+                        {"tp": partner},
+                    )
+
+    def weight_pass(n, t):
+        buf = (wl_buf, wf_buf)[n]
+        ref = buf.at[t, pl.ds(x * wh, wh)]
+        remote(ref, ref, wsend.at[n, 0], wrecv.at[n, t, x], {"tp": t}).wait_recv()
+        send(ref, ref, wfwd.at[n, 0 if t is far else 1], wrecv.at[n, t, x], to_xo)
+
+    def weight_wait(n, t, k):
+        ref = (wl_buf, wf_buf)[n].at[t, pl.ds(k * wh, wh)]
+        remote(ref, ref, wsend.at[n, 0], wrecv.at[n, t, k], to_xo).wait_recv()
+
+    def pass_up(c):
+        @pl.when(from_across(c))
+        def _():
+            kv_wait(j_xo, c)
+
+        @pl.when(not_top)
+        def _():
+            kv_copy(j_xo, c, zfwd, to_up).start()
+
+    def pass_across(c):
+        @pl.when(above0)
+        def _():
+            kv_wait(j_b, c)
+            kv_copy(j_b, c, xfwd, to_xo).start()
+
+    pass_up(via_z[0])
+    pass_across(via_x[0])
+
+    @pl.when(sp == 0)
+    def _():
+        pad[0:8, :] = jnp.zeros((8, lw), F32)
+
+    @pl.when(sp > 0)
+    def _():
+        halo_copy.wait_recv()
+        hb = halo.shape[0]
+        pad[0:8, :] = halo[...].astype(F32)[hb - 8 : hb, :]
+
+    pad[8 : 8 + rows, :] = lru_ref[...].astype(F32)
+    chans = pl.ds(pl.multiple_of(tp * lw, 128), lw)
+    taps = conv_w.shape[0]
+    taps_f32 = conv_v[:, chans].astype(F32)
+    conv = jnp.zeros((rows, lw), F32)
+    for j in range(taps):
+        conv = conv + taps_f32[j : j + 1, :] * pad[8 - (taps - 1) + j : 8 - (taps - 1) + j + rows, :]
+    conv_b = conv.astype(BF16)
+
+    def sigmoid(v):
+        return 1.0 / (1.0 + jnp.exp(-v))
+
+    recur_gate = sigmoid(jnp.dot(conv_b, bd_r[...], preferred_element_type=F32))
+    input_gate = sigmoid(jnp.dot(conv_b, bd_i[...], preferred_element_type=F32))
+    own_rate = rate_v[:, chans]
+    softplus = jnp.maximum(-own_rate, 0.0) + jnp.log1p(jnp.exp(-jnp.abs(own_rate)))
+    log_decay = -decay_sharpness * softplus * recur_gate + decay_buf[...]
+    decay = jnp.exp(log_decay)
+    driven = jnp.sqrt(one_minus_exp(2.0 * log_decay)) * input_gate * conv_b.astype(F32)
+    for n in range(lw // 128):
+        prefix_ref[n] = decay[:, n * 128 : (n + 1) * 128]
+        local_ref[n] = driven[:, n * 128 : (n + 1) * 128]
+
+    segs = 8
+    seg_len = rows // segs
+    run_a = jnp.ones((segs, lw), F32)
+    run_b = jnp.zeros((segs, lw), F32)
+    for i in range(seg_len):
+        at = pl.ds(i, segs, stride=seg_len)
+        a = [prefix_ref[n, at, :] for n in range(lw // 128)]
+        b = [local_ref[n, at, :] for n in range(lw // 128)]
+        a = jnp.concatenate(a, axis=1)
+        b = jnp.concatenate(b, axis=1)
+        run_a = run_a * a
+        run_b = a * run_b + b
+        for n in range(lw // 128):
+            prefix_ref[n, at, :] = run_a[:, n * 128 : (n + 1) * 128]
+            local_ref[n, at, :] = run_b[:, n * 128 : (n + 1) * 128]
+    seg_a[...] = run_a
+    seg_b[...] = run_b
+    end_a = seg_a[0:1, :]
+    end_b = seg_b[0:1, :]
+    for i in range(1, segs):
+        end_b = seg_a[i : i + 1, :] * end_b + seg_b[i : i + 1, :]
+        end_a = end_a * seg_a[i : i + 1, :]
+    ends[sp, 0:1, :] = end_a
+    ends[sp, 1:2, :] = end_b
+
+    def end_copy(k):
+        return remote(
+            ends.at[sp], ends.at[sp], esend.at[k], erecv.at[sp], {"sp": lax.rem(sp + k, SP)}
+        )
+
+    for k in range(1, SP):
+
+        @pl.when(sp + k < SP)
+        def _():
+            end_copy(k).start()
+
+    for c in via_z[1:]:
+        pass_up(c)
+
+    def attend(qs, st, j, lo, hi, first=False, diagonal=False, qc=half, after=None):
+        ms, os = st
+        items = [(i, h) for i in range(rows // qc) for h in range(H)]
+
+        def width(i):
+            return (lo, (i + 1) * qc) if diagonal else (lo, hi)
+
+        def scores(i, h):
+            a, b = width(i)
+            hs = slice(h * HEAD_DIM, (h + 1) * HEAD_DIM)
+            s = lax.dot_general(
+                qs[i * qc : (i + 1) * qc, hs],
+                kv_buf[j, a:b, hs],
+                (((1,), (1,)), ((), ())),
+                preferred_element_type=F32,
+            )
+            s = s * score_k - cum_buf[j, h : h + 1, a:b]
+            if diagonal:
+                causal = (
+                    lax.broadcasted_iota(jnp.int32, (qc, b - a), 0) + (i * qc - a)
+                    >= lax.broadcasted_iota(jnp.int32, (qc, b - a), 1)
+                )
+                s = jnp.where(causal, s, -1e30)
+            return s
+
+        def update(i, h, s):
+            a, b = width(i)
+            r = slice(i * qc, (i + 1) * qc)
+            top = jnp.max(s, axis=1, keepdims=True)
+            if first:
+                new = jnp.broadcast_to(top, (qc, 128))
+            else:
+                old = ms[h, r, :]
+                new = jnp.maximum(old, top)
+            ms[h, r, :] = new
+            p = jnp.exp2(s - jnp.concatenate([new] * ((b - a) // 128), axis=1)).astype(BF16)
+            v = kv_buf[j, a:b, fw + h * HEAD_DIM : fw + (h + 1) * HEAD_DIM]
+            v1 = jnp.concatenate([v, jnp.ones((b - a, 128), BF16)], axis=1)
+            pv = jnp.dot(p, v1, preferred_element_type=F32)
+            if first:
+                os[h, r, :] = pv
+            else:
+                fade = jnp.exp2(old - new)
+                os[h, r, :] = os[h, r, :] * jnp.concatenate([fade, fade], axis=1) + pv
+
+        s = scores(*items[0])
+        for n, (i, h) in enumerate(items):
+            nxt = scores(*items[n + 1]) if n + 1 < len(items) else None
+            update(i, h, s)
+            s = nxt
+            if after is not None and h == H - 1:
+                after(i)
+
+    own_st = (m_ref, o_ref)
+    far_st = (m_far, o_far)
+    up2 = {"sp": lax.rem(sp + 2 * X, SP)}
+
+    def part_copies(c):
+        return (
+            remote(part_out.at[chunk(c)], part_in.at[chunk(c)], osend.at[c, 0], orecv.at[c, 0], up2),
+            remote(stat_out.at[c], stat_in.at[c], osend.at[c, 1], orecv.at[c, 1], up2),
+        )
+
+    def send_partial(c):
+        r = slice(c * rc, (c + 1) * rc)
+        lane = lax.broadcasted_iota(jnp.int32, (rc, 128), 1)
+        stats = jnp.zeros((rc, 128), F32)
+        for h in range(H):
+            part_out[r, h * HEAD_DIM : (h + 1) * HEAD_DIM] = o_far[h, r, 0:HEAD_DIM].astype(BF16)
+            stats = jnp.where(lane == h, m_far[h, r, :], stats)
+            stats = jnp.where(lane == H + h, o_far[h, r, HEAD_DIM:], stats)
+        stat_out[c] = stats.T[0:8, :]
+        for s in part_copies(c):
+            s.start()
+
+    attend(q_ref, own_st, sp, 0, rows, True, True)
+
+    for c in via_x[1:]:
+        pass_across(c)
+
+    remote(own_cum, cum_buf.at[j_xo], csend.at[0], crecv.at[j_xo], to_xo).wait_recv()
+
+    @pl.when(helper)
+    def _():
+        for c in order:
+            q_copy(c).wait_recv()
+        attend(q_far, far_st, sp, 0, rows, True)
+
+    for c in via_x:
+
+        @pl.when(from_across(c))
+        def _():
+            kv_wait(j_xo, c)
+
+    @pl.when(helper)
+    def _():
+        attend(q_far, far_st, j_xo, 0, rows)
+
+    @pl.when(jnp.logical_and(helper, z == 0))
+    def _():
+        for c in range(CH):
+            send_partial(c)
+
+    weight_pass(0, far)
+    weight_pass(0, pfar)
+
+    @pl.when(x == 1)
+    def _():
+        attend(q_ref, own_st, j_xo, 0, rows)
+
+    @pl.when(above0)
+    def _():
+        for c in via_z:
+            kv_wait(j_b, c)
+        for j in (j_b, j_bo):
+            ref = cum_buf.at[j]
+            remote(ref, ref, csend.at[0], crecv.at[j], to_xo).wait_recv()
+
+        @pl.when(helper)
+        def _():
+            attend(q_far, far_st, j_b, 0, rows)
+
+        attend(q_ref, own_st, j_b, 0, rows)
+
+    carry_ref[0:1, :] = jnp.zeros((1, lw), F32)
+    for j in range(SP - 1):
+
+        @pl.when(j < sp)
+        def _():
+            remote(
+                ends.at[j], ends.at[j], esend.at[0], erecv.at[j], {"sp": lax.rem(sp + 1, SP)}
+            ).wait_recv()
+            carry_ref[0:1, :] = ends[j, 0:1, :] * carry_ref[0:1, :] + ends[j, 1:2, :]
+
+    carry = carry_ref[0:1, :]
+    for i in range(segs):
+        r = slice(i * seg_len, (i + 1) * seg_len)
+        g = gate_ref[r, :].astype(F32)
+        gelu = 0.5 * g * (1.0 + jnp.tanh(0.7978845608028654 * (g + 0.044715 * (g * g * g))))
+        for n in range(lw // 128):
+            cs = slice(n * 128, (n + 1) * 128)
+            states = local_ref[n, r, :] + prefix_ref[n, r, :] * carry[:, cs]
+            br_lru[tp, r, cs] = (states * gelu[:, cs]).astype(BF16)
+        if i + 1 < segs:
+            carry = seg_a[i : i + 1, :] * carry + seg_b[i : i + 1, :]
+    own_lru = br_lru.at[tp]
+    send(own_lru, own_lru, lsend.at[1], lrecv.at[tp], {"tp": far})
+    send(own_lru, own_lru, lsend.at[0], lrecv.at[tp], {"tp": partner})
+    weight_pass(1, far)
+
+    @pl.when(above0)
+    def _():
+        for c in order[0:2]:
+            kv_wait(j_bo, c)
+
+        @pl.when(helper)
+        def _():
+            attend(q_far, far_st, j_bo, half, rows)
+
+        attend(q_ref, own_st, j_bo, half, rows)
+        for c in order[2:]:
+            kv_wait(j_bo, c)
+
+        @pl.when(helper)
+        def _():
+            attend(q_far, far_st, j_bo, 0, half, qc=rc, after=send_partial)
+
+        attend(q_ref, own_st, j_bo, 0, half)
+
+    weight_pass(1, pfar)
+
+    def lru_wait(t):
+        ref = br_lru.at[t]
+        remote(ref, ref, lsend.at[0], lrecv.at[t], {"tp": partner}).wait_recv()
+
+    def pair_dot(br, buf, side, r):
+        first = 2 * side
+        return jnp.dot(br[first, r, :], buf[first], preferred_element_type=F32) + jnp.dot(
+            br[first + 1, r, :], buf[first + 1], preferred_element_type=F32
+        )
+
+    for c in own_loads:
+        c.wait()
+    for k in range(X):
+        weight_wait(0, partner, k)
+        weight_wait(1, partner, k)
+    lru_wait(partner)
+    for c in range(CH):
+        oacc[chunk(c), :] = pair_dot(br_lru, wl_buf, y, chunk(c))
+
+    for c in range(CH):
+        r = slice(c * rc, (c + 1) * rc)
+
+        @pl.when(helped)
+        def _():
+            for s in part_copies(c):
+                s.wait_recv()
+            stats = jnp.concatenate([stat_in[c], jnp.zeros((120, rc), F32)], axis=0).T
+            for h in range(H):
+                hs = slice(h * HEAD_DIM, (h + 1) * HEAD_DIM)
+                m_in = stats[:, h : h + 1]
+                l_in = stats[:, H + h : H + h + 1]
+                part = part_in[r, hs].astype(F32)
+                old = m_ref[h, r, :]
+                new = jnp.maximum(old, m_in)
+                fade = jnp.exp2(old - new)
+                grow = jnp.exp2(m_in - new)
+                total = o_ref[h, r, HEAD_DIM:] * fade + l_in * grow
+                br_fox[tp, r, hs] = (
+                    (o_ref[h, r, 0:HEAD_DIM] * fade + part * grow) / total
+                ).astype(BF16)
+
+        @pl.when(jnp.logical_not(helped))
+        def _():
+            for h in range(H):
+                hs = slice(h * HEAD_DIM, (h + 1) * HEAD_DIM)
+                br_fox[tp, r, hs] = (o_ref[h, r, 0:HEAD_DIM] / o_ref[h, r, HEAD_DIM:]).astype(BF16)
+
+        ref = br_fox.at[tp, chunk(c)]
+        send(ref, ref, fsend.at[1, c], frecv.at[tp, c], {"tp": far})
+        send(ref, ref, fsend.at[0, c], frecv.at[tp, c], {"tp": partner})
+
+    lru_wait(far)
+    ref = br_lru.at[far]
+    send(ref, ref, lfwd.at[0], lrecv.at[far], {"tp": partner})
+    for t in (far, pfar):
+        weight_wait(0, t, xo)
+    lru_wait(pfar)
+    for c in range(CH):
+        oacc[chunk(c), :] += pair_dot(br_lru, wl_buf, 1 - y, chunk(c))
+    for t in (far, pfar):
+        weight_wait(1, t, xo)
+
+    def fox_wait(src, c):
+        ref = br_fox.at[src, chunk(c)]
+        remote(ref, ref, fsend.at[0, c], frecv.at[src, c], {"tp": partner}).wait_recv()
+
+    out_copies = []
+    for c in range(CH):
+        r = chunk(c)
+        fox_wait(far, c)
+        ref = br_fox.at[far, r]
+        send(ref, ref, ffwd.at[c], frecv.at[far, c], {"tp": partner})
+        fox_wait(partner, c)
+        near = oacc[r, :] + pair_dot(br_fox, wf_buf, y, r)
+        fox_wait(pfar, c)
+        obuf[r, :] = (near + pair_dot(br_fox, wf_buf, 1 - y, r)).astype(out.dtype)
+        o = pltpu.make_async_copy(obuf.at[r], out.at[r], out_sem.at[c])
+        o.start()
+        out_copies.append(o)
+
+    for s in pending:
+        s.wait_send()
+    for c in range(CH):
+
+        @pl.when(across(c))
+        def _():
+            kv_copy(sp, c, xsend, to_xo).wait_send()
+
+        @pl.when(not_top)
+        def _():
+            kv_copy(sp, c, zsend, to_up).wait_send()
+
+        @pl.when(helped)
+        def _():
+            q_copy(c).wait_send()
+
+        @pl.when(helper)
+        def _():
+            for s in part_copies(c):
+                s.wait_send()
+
+    for c in via_z:
+
+        @pl.when(not_top)
+        def _():
+            kv_copy(j_xo, c, zfwd, to_up).wait_send()
+
+    for c in via_x:
+
+        @pl.when(above0)
+        def _():
+            kv_copy(j_b, c, xfwd, to_xo).wait_send()
+
+    @pl.when(not_top)
+    def _():
+        for c in cum_up:
+            c.wait_send()
+
+    @pl.when(sp < SP - 1)
+    def _():
+        halo_copy.wait_send()
+
+    for k in range(1, SP):
+
+        @pl.when(sp + k < SP)
+        def _():
+            end_copy(k).wait_send()
+
+    for o in out_copies:
+        o.wait()
+
+
+def block_shards(SP, TP, X, *args):
+    tokens, lru_in, gate_in, query_w = args[:4]
+    (conv_weight, rg_w, ig_w, rate, decay_extra, forget, out_lru, out_fox) = args[6:]
+    rows, dcols = tokens.shape
+    D, lw = lru_in.shape
+    fw = query_w.shape[1]
+    oc = out_lru.shape[1] // TP
+    tot = 2 * lw + 3 * fw
+    H = fw // HEAD_DIM
+    CH = 4
+    rc = rows // CH
+    bw = rg_w.shape[1]
+    hbm = pl.BlockSpec(memory_space=pl.ANY)
+    dma = pltpu.SemaphoreType.DMA
+    V = pltpu.VMEM
+    scratch = [
+        V((TP, rows, dcols), BF16),
+        V((D, tot), BF16),
+        V((2, rc, tot), F32),
+        V((2, rc, 1), F32),
+        V((rows, lw), BF16),
+        V((16, lw), BF16),
+        V((rows + 8, lw), F32),
+        V(conv_weight.shape, BF16),
+        V((lw // bw, bw, bw), BF16),
+        V((lw // bw, bw, bw), BF16),
+        V((1, rate.shape[0]), F32),
+        V((H, rows), F32),
+        V((lw, lw), BF16),
+        V((lw, lw), BF16),
+        V((rows, lw), BF16),
+        V((rows, fw), BF16),
+        V((rows, lw), F32),
+        V((lw // 128, rows, 128), F32),
+        V((lw // 128, rows, 128), F32),
+        V((8, lw), F32),
+        V((8, lw), F32),
+        V((8, lw), F32),
+        V((SP, 8, lw), F32),
+        V((SP, rows, 2 * fw), BF16),
+        V((SP, 8, rows), F32),
+        V((H, rows, 128), F32),
+        V((H, rows, 2 * HEAD_DIM), F32),
+        V((rows, fw), BF16),
+        V((H, rows, 128), F32),
+        V((H, rows, 2 * HEAD_DIM), F32),
+        V((rows, fw), BF16),
+        V((CH, 8, rc), F32),
+        V((rows, fw), BF16),
+        V((CH, 8, rc), F32),
+        V((TP, lw, oc), BF16),
+        V((TP, fw, oc), BF16),
+        V((TP, rows, lw), BF16),
+        V((TP, rows, fw), BF16),
+        V((rows, oc), F32),
+        V((rows, oc), BF16),
+        dma((14,)),
+        dma((CH,)),
+        dma((2, CH)),
+        dma((CH,)),
+        dma((TP, CH)),
+        dma((1,)),
+        dma((1,)),
+        dma((SP,)),
+        dma((SP,)),
+        dma((3,)),
+        dma((SP,)),
+        dma((CH,)),
+        dma((CH,)),
+        dma((CH,)),
+        dma((CH,)),
+        dma((SP, CH)),
+        dma((2, 4)),
+        dma((2, 2)),
+        dma((2, TP, X)),
+        dma((2,)),
+        dma((TP,)),
+        dma((2, CH)),
+        dma((CH,)),
+        dma((TP, CH)),
+        dma((1,)),
+        dma((CH,)),
+        dma((CH,)),
+        dma((CH, 2)),
+        dma((CH, 2)),
+    ]
+    return pl.pallas_call(
+        functools.partial(block_kernel, SP, TP, X, CH),
+        out_shape=jax.ShapeDtypeStruct((rows, oc), BF16),
+        in_specs=[hbm] * 14,
+        out_specs=hbm,
+        scratch_shapes=scratch,
+        compiler_params=pltpu.CompilerParams(
+            collective_id=1, has_side_effects=True, vmem_limit_bytes=60 * 1024 * 1024
+        ),
+    )(*args[:9], rate.reshape(1, -1), decay_extra, forget.T, out_lru, out_fox)
+
+
 def columns_of(mesh):
     SP = mesh.shape["sp"]
     try:
@@ -794,7 +1618,9 @@
         P("tp", None),
         P("tp", None),
     )
-    body = functools.partial(shards, mesh.shape["sp"], mesh.shape["tp"], columns_of(mesh))
+    SP, TP, X = mesh.shape["sp"], mesh.shape["tp"], columns_of(mesh)
+    small = X == 2 and TP == 4 and SP // X in (3, 4)
+    body = functools.partial(block_shards if small else shards, SP, TP, X)
     return jax.shard_map(
         body, mesh=mesh, in_specs=placed, out_specs=P("sp", "tp"), check_vma=False
     )

time: 68.7 us -> 54.7 us (0.80)
  Pallas kernels: 66.6 us -> 52.6 us
    pallas_call x1, Pallas kernels: 66.6 us -> 52.6 us  [block_shards(): pl.pallas_call(functools.partial(block_kernel, SP, TP, X, CH), out_shape=...]
where the time goes in v1:
time: 54.7 us; the launch traced here: 54.5 us
  Pallas kernels  52.6 us (96%)
  local copies, waits for them, and re-layouts  1.87 us (3%)
    pallas_call x1, Pallas kernels, block_shards(): pl.pallas_call(functools.partial(block_kernel, SP, TP, X, CH), out_shape=...  52.6 us
    unnamed x1, local copies, waits for them, and re-layouts  1.87 us

profile of v1, /device:TPU:25, one launch (start us, length us, event | category | flops | bytes accessed | tf_op | source)
XLA Modules:
  0.0 54.5 jit_solution(7300280330186375832)
XLA Ops:
  0.0 52.6 %shard_map.136 = bf16[512,512]{1,0:T(8,128)(2,1)} custom-call(bf16[512,512]{1,0:T(8,128)(2,1)} %tokens.1, bf16[2048,256]{1,0:T(8,128)(2,1)} %lru_in.1, bf16[2048,256]{1,0:T(8,128)(2,1)} %gate_in.1, bf16[2048,256]{1,0:T(8,128)(2,1)} %query_w.1, bf16[2048,256]{1,0:T(8,128)(2,1)} %key_w.1, bf16[2048,256]{1,0:T(8,128)(2,1)} %value_w.1, bf16[4,1024]{1,0:T(4,128)(2,1)} %conv_w.1, ...), custom_call_target="tpu_custom_call" | custom-call | tf_op jit(solution)/shard_map/pallas_call | solution.py:1583
  52.6 1.9 %copy.16 = bf16[512,512]{1,0:T(8,128)(2,1)} copy(bf16[512,512]{1,0:T(8,128)(2,1)} %shard_map.136) | data formatting | bytes 1048576

commit v2 on v1

--- a/solution.py
+++ b/solution.py
@@ -830,11 +830,8 @@
     br_lru,
     br_fox,
     oacc,
-    obuf,
     load_sem,
-    out_sem,
     tsend,
-    tfwd,
     trecv,
     hsend,
     hrecv,
@@ -848,14 +845,12 @@
     xfwd,
     kvrecv,
     wsend,
-    wfwd,
+    wrecv_own,
     wrecv,
     lsend,
     lrecv,
     fsend,
-    ffwd,
     frecv,
-    lfwd,
     qsend,
     qrecv,
     osend,
@@ -889,8 +884,14 @@
     not_top = z < Z - 1
     above0 = z >= 1
     order = list(range(CH - 1, -1, -1))
-    via_z = order[0::2]
-    via_x = order[1::2]
+    via_x = order[0::2]
+    via_z = order[1::2]
+    goes_up = jnp.logical_and(not_top, z != Z - 3)
+    all_over_x = z == Z - 2
+    whalf = lax.rem(x + z, X)
+    odd = lax.rem(z, 2) == 1
+    PARTNER, FAR, PFAR = 0, 1, 2
+    ACROSS, BELOW, DIAG = 0, 1, 2
     score_k = HEAD_DIM ** (-0.5) * LOG2E
 
     def chunk(c):
@@ -911,57 +912,55 @@
         c.start()
         return c
 
-    tok_load = load(0, tokens, tok_buf.at[tp])
+    tok_loads = [
+        load(n, tokens.at[chunk(c)], tok_buf.at[tp, chunk(c)]) for n, c in enumerate(order)
+    ]
     cols = (0, fw, 2 * fw, 2 * fw + lw, 3 * fw + lw, 3 * fw + 2 * lw)
-    w_loads = [
-        load(1 + i, w, w_buf.at[:, cols[i] : cols[i + 1]])
-        for i, w in enumerate((key_w, value_w, lru_in, query_w, gate_in))
-    ]
+    for i, w in enumerate((key_w, value_w, lru_in, query_w, gate_in)):
+        load(CH, w, w_buf.at[:, cols[i] : cols[i + 1]])
     mine = pl.ds(pl.multiple_of(tp * oc, 128), oc)
     bw = rg_w.shape[1]
     nb = lw // bw
     gates = pl.ds(tp * nb, nb)
-    forget_load = load(6, forget, forget_v)
+    forget_load = load(CH + 1, forget, forget_v)
     small_loads = [
-        load(7, conv_w, conv_v),
-        load(8, rg_w.at[gates], rg_v),
-        load(9, ig_w.at[gates], ig_v),
-        load(10, rate, rate_v),
-        load(11, decay_extra, decay_buf),
+        load(CH + 2, conv_w, conv_v),
+        load(CH + 3, rg_w.at[gates], rg_v),
+        load(CH + 4, ig_w.at[gates], ig_v),
+        load(CH + 5, rate, rate_v),
+        load(CH + 6, decay_extra, decay_buf),
     ]
     own_loads = [
-        load(12, out_lru.at[:, mine], wl_buf.at[tp]),
-        load(13, out_fox.at[:, mine], wf_buf.at[tp]),
+        load(CH + 7, out_lru.at[:, mine], wl_buf.at[tp]),
+        load(CH + 8, out_fox.at[:, mine], wf_buf.at[tp]),
     ]
-    tok_load.wait()
     pl.semaphore_wait(barrier, SP - 1 + TP - 1)
 
-    pending = []
-
-    def send(src, dst, send_sem, recv_sem, device):
-        s = remote(src, dst, send_sem, recv_sem, device)
-        s.start()
-        pending.append(s)
-
-    for c in order:
+    def send(ref, send_sem, recv_sem, device):
+        remote(ref, ref, send_sem, recv_sem, device).start()
+
+    def arrived(ref, recv_sem):
+        remote(ref, ref, recv_sem, recv_sem, to_xo).wait_recv()
+
+    def sent(ref, send_sem):
+        remote(ref, ref, send_sem, send_sem, to_xo).wait_send()
+
+    for n, c in enumerate(order):
+        tok_loads[n].wait()
         ref = tok_buf.at[tp, chunk(c)]
-        send(ref, ref, tsend.at[1, c], trecv.at[tp, c], {"tp": far})
-        send(ref, ref, tsend.at[0, c], trecv.at[tp, c], {"tp": partner})
+        send(ref, tsend.at[0], trecv.at[FAR, c], {"tp": far})
+        send(ref, tsend.at[1], trecv.at[PARTNER, c], {"tp": partner})
 
     forget_load.wait()
     cum_buf[sp] = jnp.zeros_like(cum_buf[sp])
     cum_buf[sp, 0:H, :] = forget_v[...] * LOG2E
     own_cum = cum_buf.at[sp]
-    send(own_cum, own_cum, csend.at[0], crecv.at[sp], to_xo)
-    cum_up = (
-        remote(own_cum, own_cum, csend.at[1], crecv.at[sp], to_up),
-        remote(own_cum, own_cum, csend.at[2], crecv.at[sp], {"sp": lax.rem(j_xo + X, SP)}),
-    )
+    send(own_cum, csend.at[0], crecv.at[ACROSS], to_xo)
 
     @pl.when(not_top)
     def _():
-        for c in cum_up:
-            c.start()
+        send(own_cum, csend.at[1], crecv.at[BELOW], to_up)
+        send(own_cum, csend.at[1], crecv.at[DIAG], {"sp": lax.rem(j_xo + X, SP)})
 
     for c in small_loads:
         c.wait()
@@ -971,12 +970,10 @@
         sl = pl.ds(n * bw, bw)
         bd_r[sl, sl] = rg_v[n]
         bd_i[sl, sl] = ig_v[n]
-    for c in w_loads:
-        c.wait()
-
-    def tok_wait(src, c):
-        ref = tok_buf.at[src, chunk(c)]
-        remote(ref, ref, tsend.at[0, c], trecv.at[src, c], {"tp": partner}).wait_recv()
+    pltpu.make_async_copy(w_buf, w_buf, load_sem.at[CH]).wait()
+
+    def tok_wait(src, role, c):
+        arrived(tok_buf.at[src, chunk(c)], trecv.at[role, c])
 
     def features(side, c):
         first = 2 * side
@@ -990,7 +987,7 @@
         return jnp.sum(v32 * v32, axis=1, keepdims=True)
 
     def near_part(c, slot):
-        tok_wait(partner, c)
+        tok_wait(partner, PARTNER, c)
         v = features(y, c)
         sq[slot] = squares(v)
         acc[slot] = jnp.dot(v, w_buf[w_rows(y), :], preferred_element_type=F32)
@@ -1003,35 +1000,36 @@
         {"sp": lax.rem(sp + 1, SP)},
     )
 
-    def kv_copy(j, c, send_sem, device):
-        ref = kv_buf.at[j, chunk(c)]
-        return remote(ref, ref, send_sem.at[c], kvrecv.at[j, c], device)
-
-    def kv_wait(j, c):
-        kv_copy(j, c, zsend, to_up).wait_recv()
-
-    def across(c):
-        return jnp.logical_or(x == 0, z <= (Z - 2 if c in via_z else Z - 3))
-
-    def from_across(c):
-        return jnp.logical_or(x == 1, z <= (Z - 2 if c in via_z else Z - 3))
+    def kv_send(j, c, send_sem, role, device):
+        send(kv_buf.at[j, chunk(c)], send_sem.at[0], kvrecv.at[role, c], device)
+
+    def kv_wait(j, c, role):
+        arrived(kv_buf.at[j, chunk(c)], kvrecv.at[role, c])
+
+    def all_across(own_x):
+        return jnp.logical_or(own_x, helper)
+
+    def across(own_x, c):
+        need = all_across(own_x)
+        return jnp.logical_or(need, goes_up) if c in via_z else need
 
     def q_copy(c):
         return remote(
             q_ref.at[chunk(c)],
             q_far.at[chunk(c)],
-            qsend.at[c],
-            qrecv.at[c],
+            qsend.at[0],
+            qrecv.at[0],
             {"sp": lax.rem(sp + SP - 2 * X, SP)},
         )
 
     def far_part(i, c, slot):
-        tok_wait(far, c)
-        ref = tok_buf.at[far, chunk(c)]
-        send(ref, ref, tfwd.at[c], trecv.at[far, c], {"tp": partner})
+        tok_wait(far, FAR, c)
+        send(tok_buf.at[far, chunk(c)], tsend.at[2], trecv.at[PFAR, c], {"tp": partner})
         if i + 1 < CH:
             near_part(order[i + 1], 1 - slot)
-        tok_wait(pfar, c)
+        tok_wait(pfar, PFAR, c)
+        if i == CH - 1:
+            send_weights()
         v = features(1 - y, c)
         row_scale = lax.rsqrt((sq[slot] + squares(v)) / D + epsilon_norm)
 
@@ -1042,13 +1040,13 @@
 
         kv_buf[sp, chunk(c), :] = part(0, 2)
 
-        @pl.when(across(c))
-        def _():
-            kv_copy(sp, c, xsend, to_xo).start()
+        @pl.when(across(x == 0, c))
+        def _():
+            kv_send(sp, c, xsend, ACROSS, to_xo)
 
         @pl.when(not_top)
         def _():
-            kv_copy(sp, c, zsend, to_up).start()
+            kv_send(sp, c, zsend, BELOW, to_up)
 
         rest = part(2, 5)
         lru_ref[chunk(c), :] = rest[:, 0:lw]
@@ -1065,59 +1063,57 @@
             def _():
                 halo_copy.start()
 
-    def weight_copy(i, w, buf, t, k):
-        r = pl.ds(x * wh, wh)
-        c = pl.ds(pl.multiple_of(t * oc, 128), oc)
-        return remote(w.at[r, c], buf.at[tp, r], wsend.at[i, k], wrecv.at[i, tp, x], {"tp": t})
+    banks = ((out_lru, wl_buf), (out_fox, wf_buf))
+
+    def send_weights():
+        r = pl.ds(pl.multiple_of(whalf * wh, wh), wh)
+        for n, (w, buf) in enumerate(banks):
+            for role, t in ((FAR, far), (PFAR, pfar)):
+                c = pl.ds(pl.multiple_of(t * oc, 128), oc)
+                remote(
+                    w.at[r, c], buf.at[tp, r], wsend.at[0], wrecv.at[n, role - 1, whalf], {"tp": t}
+                ).start()
+        c = pl.ds(pl.multiple_of(partner * oc, 128), oc)
+        for n, (w, buf) in enumerate(banks):
+            remote(w.at[:, c], buf.at[tp], wsend.at[1], wrecv_own.at[n], {"tp": partner}).start()
+
+    def weight_part(n, role, k):
+        t = far if role == FAR else pfar
+        ref = banks[n][1].at[t, pl.ds(pl.multiple_of(k * wh, wh), wh)]
+        return ref, wrecv.at[n, role - 1, k]
+
+    def weight_pass(n, role):
+        ref, sem = weight_part(n, role, whalf)
+        arrived(ref, sem)
+
+        @pl.when(odd)
+        def _():
+            send(ref, wsend.at[2], sem, to_xo)
+            send(ref, wsend.at[3], sem, {"sp": lax.rem(sp + SP - X, SP)})
+
+    def weight_wait(n, role):
+        arrived(*weight_part(n, role, 1 - whalf))
+
+    def pass_up(c):
+        @pl.when(goes_up)
+        def _():
+            kv_wait(j_xo, c, ACROSS)
+            kv_send(j_xo, c, zfwd, DIAG, to_up)
+
+    def pass_across(c):
+        @pl.when(above0 if c in via_x else all_over_x)
+        def _():
+            kv_wait(j_b, c, BELOW)
+            kv_send(j_b, c, xfwd, DIAG, to_xo)
 
     near_part(order[0], 0)
     for i, c in enumerate(order):
         far_part(i, c, i % 2)
         if i == CH - 2:
-            for n, (w, buf) in enumerate(((out_lru, wl_buf), (out_fox, wf_buf))):
-                for k, t in enumerate((far, pfar)):
-                    s = weight_copy(n, w, buf, t, k)
-                    s.start()
-                    pending.append(s)
-            for n, (w, buf) in enumerate(((out_lru, wl_buf), (out_fox, wf_buf))):
-                c2 = pl.ds(pl.multiple_of(partner * oc, 128), oc)
-                for k in range(X):
-                    r = pl.ds(k * wh, wh)
-                    send(
-                        w.at[r, c2],
-                        buf.at[tp, r],
-                        wsend.at[n, 2 + k],
-                        wrecv.at[n, tp, k],
-                        {"tp": partner},
-                    )
-
-    def weight_pass(n, t):
-        buf = (wl_buf, wf_buf)[n]
-        ref = buf.at[t, pl.ds(x * wh, wh)]
-        remote(ref, ref, wsend.at[n, 0], wrecv.at[n, t, x], {"tp": t}).wait_recv()
-        send(ref, ref, wfwd.at[n, 0 if t is far else 1], wrecv.at[n, t, x], to_xo)
-
-    def weight_wait(n, t, k):
-        ref = (wl_buf, wf_buf)[n].at[t, pl.ds(k * wh, wh)]
-        remote(ref, ref, wsend.at[n, 0], wrecv.at[n, t, k], to_xo).wait_recv()
-
-    def pass_up(c):
-        @pl.when(from_across(c))
-        def _():
-            kv_wait(j_xo, c)
-
-        @pl.when(not_top)
-        def _():
-            kv_copy(j_xo, c, zfwd, to_up).start()
-
-    def pass_across(c):
-        @pl.when(above0)
-        def _():
-            kv_wait(j_b, c)
-            kv_copy(j_b, c, xfwd, to_xo).start()
-
-    pass_up(via_z[0])
-    pass_across(via_x[0])
+            pass_across(order[0])
+
+    pass_up(order[1])
+    pass_across(order[1])
 
     @pl.when(sp == 0)
     def _():
@@ -1179,7 +1175,11 @@
 
     def end_copy(k):
         return remote(
-            ends.at[sp], ends.at[sp], esend.at[k], erecv.at[sp], {"sp": lax.rem(sp + k, SP)}
+            ends.at[sp],
+            ends.at[sp],
+            esend.at[k - 1],
+            erecv.at[lax.rem(sp, SP - 1)],
+            {"sp": lax.rem(sp + k, SP)},
         )
 
     for k in range(1, SP):
@@ -1188,8 +1188,7 @@
         def _():
             end_copy(k).start()
 
-    for c in via_z[1:]:
-        pass_up(c)
+    pass_across(order[2])
 
     def attend(qs, st, j, lo, hi, first=False, diagonal=False, qc=half, after=None):
         ms, os = st
@@ -1250,8 +1249,8 @@
 
     def part_copies(c):
         return (
-            remote(part_out.at[chunk(c)], part_in.at[chunk(c)], osend.at[c, 0], orecv.at[c, 0], up2),
-            remote(stat_out.at[c], stat_in.at[c], osend.at[c, 1], orecv.at[c, 1], up2),
+            remote(part_out.at[chunk(c)], part_in.at[chunk(c)], osend.at[0], orecv.at[c, 0], up2),
+            remote(stat_out.at[c], stat_in.at[c], osend.at[1], orecv.at[c, 1], up2),
         )
 
     def send_partial(c):
@@ -1268,22 +1267,24 @@
 
     attend(q_ref, own_st, sp, 0, rows, True, True)
 
-    for c in via_x[1:]:
-        pass_across(c)
-
-    remote(own_cum, cum_buf.at[j_xo], csend.at[0], crecv.at[j_xo], to_xo).wait_recv()
+    pass_up(order[3])
+    pass_across(order[3])
+
+    arrived(cum_buf.at[j_xo], crecv.at[ACROSS])
 
     @pl.when(helper)
     def _():
-        for c in order:
-            q_copy(c).wait_recv()
+        arrived(q_far, qrecv.at[0])
         attend(q_far, far_st, sp, 0, rows, True)
 
-    for c in via_x:
-
-        @pl.when(from_across(c))
-        def _():
-            kv_wait(j_xo, c)
+    for c in order:
+        need = all_across(x == 1)
+        if c in via_z:
+            need = jnp.logical_and(need, jnp.logical_not(goes_up))
+
+        @pl.when(need)
+        def _():
+            kv_wait(j_xo, c, ACROSS)
 
     @pl.when(helper)
     def _():
@@ -1294,8 +1295,23 @@
         for c in range(CH):
             send_partial(c)
 
-    weight_pass(0, far)
-    weight_pass(0, pfar)
+    @pl.when(above0)
+    def _():
+        for c in via_z:
+
+            @pl.when(jnp.logical_not(all_over_x))
+            def _():
+                kv_wait(j_b, c, BELOW)
+
+        arrived(cum_buf.at[j_b], crecv.at[BELOW])
+        arrived(cum_buf.at[j_bo], crecv.at[DIAG])
+
+    @pl.when(jnp.logical_and(helper, above0))
+    def _():
+        attend(q_far, far_st, j_b, 0, rows)
+
+    weight_pass(0, FAR)
+    weight_pass(0, PFAR)
 
     @pl.when(x == 1)
     def _():
@@ -1303,16 +1319,6 @@
 
     @pl.when(above0)
     def _():
-        for c in via_z:
-            kv_wait(j_b, c)
-        for j in (j_b, j_bo):
-            ref = cum_buf.at[j]
-            remote(ref, ref, csend.at[0], crecv.at[j], to_xo).wait_recv()
-
-        @pl.when(helper)
-        def _():
-            attend(q_far, far_st, j_b, 0, rows)
-
         attend(q_ref, own_st, j_b, 0, rows)
 
     carry_ref[0:1, :] = jnp.zeros((1, lw), F32)
@@ -1320,9 +1326,7 @@
 
         @pl.when(j < sp)
         def _():
-            remote(
-                ends.at[j], ends.at[j], esend.at[0], erecv.at[j], {"sp": lax.rem(sp + 1, SP)}
-            ).wait_recv()
+            arrived(ends.at[j], erecv.at[j])
             carry_ref[0:1, :] = ends[j, 0:1, :] * carry_ref[0:1, :] + ends[j, 1:2, :]
 
     carry = carry_ref[0:1, :]
@@ -1337,34 +1341,31 @@
         if i + 1 < segs:
             carry = seg_a[i : i + 1, :] * carry + seg_b[i : i + 1, :]
     own_lru = br_lru.at[tp]
-    send(own_lru, own_lru, lsend.at[1], lrecv.at[tp], {"tp": far})
-    send(own_lru, own_lru, lsend.at[0], lrecv.at[tp], {"tp": partner})
-    weight_pass(1, far)
+    send(own_lru, lsend.at[0], lrecv.at[FAR], {"tp": far})
+    send(own_lru, lsend.at[0], lrecv.at[PARTNER], {"tp": partner})
+    weight_pass(1, FAR)
 
     @pl.when(above0)
     def _():
         for c in order[0:2]:
-            kv_wait(j_bo, c)
+            kv_wait(j_bo, c, DIAG)
 
         @pl.when(helper)
         def _():
             attend(q_far, far_st, j_bo, half, rows)
 
-        attend(q_ref, own_st, j_bo, half, rows)
         for c in order[2:]:
-            kv_wait(j_bo, c)
+            kv_wait(j_bo, c, DIAG)
 
         @pl.when(helper)
         def _():
             attend(q_far, far_st, j_bo, 0, half, qc=rc, after=send_partial)
 
-        attend(q_ref, own_st, j_bo, 0, half)
-
-    weight_pass(1, pfar)
-
-    def lru_wait(t):
-        ref = br_lru.at[t]
-        remote(ref, ref, lsend.at[0], lrecv.at[t], {"tp": partner}).wait_recv()
+    weight_pass(1, PFAR)
+
+    @pl.when(above0)
+    def _():
+        attend(q_ref, own_st, j_bo, 0, rows)
 
     def pair_dot(br, buf, side, r):
         first = 2 * side
@@ -1374,10 +1375,9 @@
 
     for c in own_loads:
         c.wait()
-    for k in range(X):
-        weight_wait(0, partner, k)
-        weight_wait(1, partner, k)
-    lru_wait(partner)
+    for n in range(2):
+        arrived(banks[n][1].at[partner], wrecv_own.at[n])
+    arrived(br_lru.at[partner], lrecv.at[PARTNER])
     for c in range(CH):
         oacc[chunk(c), :] = pair_dot(br_lru, wl_buf, y, chunk(c))
 
@@ -1410,75 +1410,85 @@
                 br_fox[tp, r, hs] = (o_ref[h, r, 0:HEAD_DIM] / o_ref[h, r, HEAD_DIM:]).astype(BF16)
 
         ref = br_fox.at[tp, chunk(c)]
-        send(ref, ref, fsend.at[1, c], frecv.at[tp, c], {"tp": far})
-        send(ref, ref, fsend.at[0, c], frecv.at[tp, c], {"tp": partner})
-
-    lru_wait(far)
-    ref = br_lru.at[far]
-    send(ref, ref, lfwd.at[0], lrecv.at[far], {"tp": partner})
-    for t in (far, pfar):
-        weight_wait(0, t, xo)
-    lru_wait(pfar)
+        send(ref, fsend.at[0], frecv.at[FAR, c], {"tp": far})
+        send(ref, fsend.at[1], frecv.at[PARTNER, c], {"tp": partner})
+
+    arrived(br_lru.at[far], lrecv.at[FAR])
+    send(br_lru.at[far], lsend.at[1], lrecv.at[PFAR], {"tp": partner})
+    for role in (FAR, PFAR):
+        weight_wait(0, role)
+        weight_wait(1, role)
+    arrived(br_lru.at[pfar], lrecv.at[PFAR])
     for c in range(CH):
         oacc[chunk(c), :] += pair_dot(br_lru, wl_buf, 1 - y, chunk(c))
-    for t in (far, pfar):
-        weight_wait(1, t, xo)
-
-    def fox_wait(src, c):
-        ref = br_fox.at[src, chunk(c)]
-        remote(ref, ref, fsend.at[0, c], frecv.at[src, c], {"tp": partner}).wait_recv()
-
-    out_copies = []
+
+    def fox_wait(src, role, c):
+        arrived(br_fox.at[src, chunk(c)], frecv.at[role, c])
+
+    def fox_pass(c):
+        fox_wait(far, FAR, c)
+        send(br_fox.at[far, chunk(c)], fsend.at[2], frecv.at[PFAR, c], {"tp": partner})
+
+    fox_pass(0)
     for c in range(CH):
         r = chunk(c)
-        fox_wait(far, c)
-        ref = br_fox.at[far, r]
-        send(ref, ref, ffwd.at[c], frecv.at[far, c], {"tp": partner})
-        fox_wait(partner, c)
-        near = oacc[r, :] + pair_dot(br_fox, wf_buf, y, r)
-        fox_wait(pfar, c)
-        obuf[r, :] = (near + pair_dot(br_fox, wf_buf, 1 - y, r)).astype(out.dtype)
-        o = pltpu.make_async_copy(obuf.at[r], out.at[r], out_sem.at[c])
-        o.start()
-        out_copies.append(o)
-
-    for s in pending:
-        s.wait_send()
-    for c in range(CH):
-
-        @pl.when(across(c))
-        def _():
-            kv_copy(sp, c, xsend, to_xo).wait_send()
-
-        @pl.when(not_top)
-        def _():
-            kv_copy(sp, c, zsend, to_up).wait_send()
-
-        @pl.when(helped)
-        def _():
-            q_copy(c).wait_send()
-
-        @pl.when(helper)
-        def _():
-            for s in part_copies(c):
-                s.wait_send()
-
-    for c in via_z:
-
-        @pl.when(not_top)
-        def _():
-            kv_copy(j_xo, c, zfwd, to_up).wait_send()
-
-    for c in via_x:
-
-        @pl.when(above0)
-        def _():
-            kv_copy(j_b, c, xfwd, to_xo).wait_send()
+        if c + 1 < CH:
+            fox_pass(c + 1)
+        fox_wait(partner, PARTNER, c)
+        oacc[r, :] += pair_dot(br_fox, wf_buf, y, r)
+        fox_wait(pfar, PFAR, c)
+        out[r, :] = (oacc[r, :] + pair_dot(br_fox, wf_buf, 1 - y, r)).astype(out.dtype)
+
+    for k in range(3):
+        sent(tok_buf.at[0], tsend.at[k])
+        sent(br_fox.at[0], fsend.at[k])
+    sent(br_lru.at[pl.ds(0, 2)], lsend.at[0])
+    sent(br_lru.at[0], lsend.at[1])
+    for k in range(2):
+        sent(wl_buf.at[pl.ds(0, 2)], wsend.at[k])
+
+    @pl.when(odd)
+    def _():
+        for k in range(2, 4):
+            sent(wl_buf.at[pl.ds(0, 2)], wsend.at[k])
+
+    sent(own_cum, csend.at[0])
+    top_half = pl.ds(0, half)
+    need = all_across(x == 0)
+
+    @pl.when(need)
+    def _():
+        sent(kv_buf.at[0], xsend.at[0])
+
+    @pl.when(jnp.logical_and(goes_up, jnp.logical_not(need)))
+    def _():
+        sent(kv_buf.at[0, top_half], xsend.at[0])
+
+    @pl.when(goes_up)
+    def _():
+        sent(kv_buf.at[0, top_half], zfwd.at[0])
+
+    @pl.when(all_over_x)
+    def _():
+        sent(kv_buf.at[0], xfwd.at[0])
+
+    @pl.when(jnp.logical_and(above0, jnp.logical_not(all_over_x)))
+    def _():
+        sent(kv_buf.at[0, top_half], xfwd.at[0])
 
     @pl.when(not_top)
     def _():
-        for c in cum_up:
-            c.wait_send()
+        sent(kv_buf.at[0], zsend.at[0])
+        sent(cum_buf.at[pl.ds(0, 2)], csend.at[1])
+
+    @pl.when(helped)
+    def _():
+        sent(q_ref, qsend.at[0])
+
+    @pl.when(helper)
+    def _():
+        sent(part_out, osend.at[0])
+        sent(stat_out, osend.at[1])
 
     @pl.when(sp < SP - 1)
     def _():
@@ -1489,9 +1499,6 @@
         @pl.when(sp + k < SP)
         def _():
             end_copy(k).wait_send()
-
-    for o in out_copies:
-        o.wait()
 
 
 def block_shards(SP, TP, X, *args):
@@ -1549,42 +1556,37 @@
         V((TP, rows, lw), BF16),
         V((TP, rows, fw), BF16),
         V((rows, oc), F32),
-        V((rows, oc), BF16),
-        dma((14,)),
-        dma((CH,)),
-        dma((2, CH)),
-        dma((CH,)),
-        dma((TP, CH)),
+        dma((CH + 9,)),
+        dma((3,)),
+        dma((3, CH)),
         dma((1,)),
         dma((1,)),
-        dma((SP,)),
-        dma((SP,)),
+        dma((SP - 1,)),
+        dma((SP - 1,)),
+        dma((2,)),
         dma((3,)),
-        dma((SP,)),
-        dma((CH,)),
-        dma((CH,)),
-        dma((CH,)),
-        dma((CH,)),
-        dma((SP, CH)),
-        dma((2, 4)),
-        dma((2, 2)),
-        dma((2, TP, X)),
+        dma((1,)),
+        dma((1,)),
+        dma((1,)),
+        dma((1,)),
+        dma((3, CH)),
+        dma((4,)),
         dma((2,)),
-        dma((TP,)),
-        dma((2, CH)),
-        dma((CH,)),
-        dma((TP, CH)),
+        dma((2, 2, X)),
+        dma((2,)),
+        dma((3,)),
+        dma((3,)),
+        dma((3, CH)),
         dma((1,)),
-        dma((CH,)),
-        dma((CH,)),
-        dma((CH, 2)),
+        dma((1,)),
+        dma((2,)),
         dma((CH, 2)),
     ]
     return pl.pallas_call(
         functools.partial(block_kernel, SP, TP, X, CH),
-        out_shape=jax.ShapeDtypeStruct((rows, oc), BF16),
+        out_shape=pltpu.VMEM((rows, oc), BF16),
         in_specs=[hbm] * 14,
-        out_specs=hbm,
+        out_specs=pl.BlockSpec(memory_space=pltpu.VMEM),
         scratch_shapes=scratch,
         compiler_params=pltpu.CompilerParams(
             collective_id=1, has_side_effects=True, vmem_limit_bytes=60 * 1024 * 1024
@@ -1619,7 +1621,7 @@
         P("tp", None),
     )
     SP, TP, X = mesh.shape["sp"], mesh.shape["tp"], columns_of(mesh)
-    small = X == 2 and TP == 4 and SP // X in (3, 4)
+    small = X == 2 and TP == 4 and SP // X == 4
     body = functools.partial(block_shards if small else shards, SP, TP, X)
     return jax.shard_map(
         body, mesh=mesh, in_specs=placed, out_specs=P("sp", "tp"), check_vma=False

time: 54.7 us -> 50 us (0.914)
  Pallas kernels: 52.6 us -> 49 us
  local copies, waits for them, and re-layouts: 1.87 us -> 0.8 us
    pallas_call x1, Pallas kernels: 52.6 us -> 49 us  [block_shards(): pl.pallas_call(functools.partial(block_kernel, SP, TP, X, CH), out_shape=...]
    unnamed x1, local copies, waits for them, and re-layouts: 1.87 us -> 0.8 us
where the time goes in v2:
time: 50 us; the launch traced here: 49.8 us
  Pallas kernels  49 us (98%)
  local copies, waits for them, and re-layouts  0.8 us (2%)
    pallas_call x1, Pallas kernels, block_shards(): pl.pallas_call(functools.partial(block_kernel, SP, TP, X, CH), out_shape=...  49 us

profile of v2, /device:TPU:25, one launch (start us, length us, event | category | flops | bytes accessed | tf_op | source)
XLA Modules:
  0.0 49.8 jit_solution(7958056945446859047)
XLA Ops:
  0.0 49.0 %shard_map.136 = bf16[512,512]{1,0:T(8,128)(2,1)S(1)} custom-call(bf16[512,512]{1,0:T(8,128)(2,1)} %tokens.1, bf16[2048,256]{1,0:T(8,128)(2,1)} %lru_in.1, bf16[2048,256]{1,0:T(8,128)(2,1)} %gate_in.1, bf16[2048,256]{1,0:T(8,128)(2,1)} %query_w.1, bf16[2048,256]{1,0:T(8,128)(2,1)} %key_w.1, bf16[2048,256]{1,0:T(8,128)(2,1)} %value_w.1, ...), custom_call_target="tpu_custom_call" | custom-call | tf_op jit(solution)/shard_map/pallas_call | solution.py:1585
  49.0 0.8 %copy.16 = bf16[512,512]{1,0:T(8,128)(2,1)} copy(bf16[512,512]{1,0:T(8,128)(2,1)S(1)} %shard_map.136) | data formatting | bytes 1048576

commit v3 on v2

--- a/solution.py
+++ b/solution.py
@@ -884,12 +884,16 @@
     not_top = z < Z - 1
     above0 = z >= 1
     order = list(range(CH - 1, -1, -1))
-    via_x = order[0::2]
-    via_z = order[1::2]
-    goes_up = jnp.logical_and(not_top, z != Z - 3)
-    all_over_x = z == Z - 2
+    second_top = z == Z - 2
+    climbs = {order[1]: not_top, order[3]: second_top}
+    crosses = {
+        order[0]: above0,
+        order[2]: above0,
+        order[3]: jnp.logical_and(above0, not_top),
+    }
     whalf = lax.rem(x + z, X)
-    odd = lax.rem(z, 2) == 1
+    top = z == Z - 1
+    first_core = lax.rem(tp, 2) == 0
     PARTNER, FAR, PFAR = 0, 1, 2
     ACROSS, BELOW, DIAG = 0, 1, 2
     score_k = HEAD_DIM ** (-0.5) * LOG2E
@@ -952,8 +956,7 @@
         send(ref, tsend.at[1], trecv.at[PARTNER, c], {"tp": partner})
 
     forget_load.wait()
-    cum_buf[sp] = jnp.zeros_like(cum_buf[sp])
-    cum_buf[sp, 0:H, :] = forget_v[...] * LOG2E
+    cum_buf[sp] = forget_v[...] * LOG2E
     own_cum = cum_buf.at[sp]
     send(own_cum, csend.at[0], crecv.at[ACROSS], to_xo)
 
@@ -1011,14 +1014,14 @@
 
     def across(own_x, c):
         need = all_across(own_x)
-        return jnp.logical_or(need, goes_up) if c in via_z else need
+        return jnp.logical_or(need, climbs[c]) if c in climbs else need
 
     def q_copy(c):
         return remote(
             q_ref.at[chunk(c)],
             q_far.at[chunk(c)],
             qsend.at[0],
-            qrecv.at[0],
+            qrecv.at[0 if c in order[0:2] else 1],
             {"sp": lax.rem(sp + SP - 2 * X, SP)},
         )
 
@@ -1067,15 +1070,20 @@
 
     def send_weights():
         r = pl.ds(pl.multiple_of(whalf * wh, wh), wh)
-        for n, (w, buf) in enumerate(banks):
+
+        def over_y(n):
+            w, buf = banks[n]
             for role, t in ((FAR, far), (PFAR, pfar)):
                 c = pl.ds(pl.multiple_of(t * oc, 128), oc)
                 remote(
-                    w.at[r, c], buf.at[tp, r], wsend.at[0], wrecv.at[n, role - 1, whalf], {"tp": t}
+                    w.at[r, c], buf.at[tp, r], wsend.at[n], wrecv.at[n, role - 1, whalf], {"tp": t}
                 ).start()
+
+        pl.when(above0)(lambda: over_y(0))
+        over_y(1)
         c = pl.ds(pl.multiple_of(partner * oc, 128), oc)
         for n, (w, buf) in enumerate(banks):
-            remote(w.at[:, c], buf.at[tp], wsend.at[1], wrecv_own.at[n], {"tp": partner}).start()
+            remote(w.at[:, c], buf.at[tp], wsend.at[2], wrecv_own.at[n], {"tp": partner}).start()
 
     def weight_part(n, role, k):
         t = far if role == FAR else pfar
@@ -1084,24 +1092,44 @@
 
     def weight_pass(n, role):
         ref, sem = weight_part(n, role, whalf)
-        arrived(ref, sem)
-
-        @pl.when(odd)
-        def _():
-            send(ref, wsend.at[2], sem, to_xo)
+
+        def take():
+            arrived(ref, sem)
+
+        if n == 0:
+            pl.when(above0)(take)
+        else:
+            take()
+
+        @pl.when(above0)
+        def _():
             send(ref, wsend.at[3], sem, {"sp": lax.rem(sp + SP - X, SP)})
 
+        @pl.when(top)
+        def _():
+            send(ref, wsend.at[4], sem, to_xo)
+
+    def weight_pass_bottom(role):
+        @pl.when(z == 0)
+        def _():
+            ref, sem = weight_part(0, role, 1 - whalf)
+            arrived(ref, sem)
+            send(ref, wsend.at[4], sem, to_xo)
+
     def weight_wait(n, role):
-        arrived(*weight_part(n, role, 1 - whalf))
+        k = 1 - whalf
+        if n == 0:
+            k = jnp.where(z == 0, whalf, k)
+        arrived(*weight_part(n, role, k))
 
     def pass_up(c):
-        @pl.when(goes_up)
+        @pl.when(climbs[c])
         def _():
             kv_wait(j_xo, c, ACROSS)
             kv_send(j_xo, c, zfwd, DIAG, to_up)
 
     def pass_across(c):
-        @pl.when(above0 if c in via_x else all_over_x)
+        @pl.when(crosses[c])
         def _():
             kv_wait(j_b, c, BELOW)
             kv_send(j_b, c, xfwd, DIAG, to_xo)
@@ -1109,11 +1137,9 @@
     near_part(order[0], 0)
     for i, c in enumerate(order):
         far_part(i, c, i % 2)
-        if i == CH - 2:
-            pass_across(order[0])
-
+
+    pass_across(order[0])
     pass_up(order[1])
-    pass_across(order[1])
 
     @pl.when(sp == 0)
     def _():
@@ -1182,17 +1208,19 @@
             {"sp": lax.rem(sp + k, SP)},
         )
 
-    for k in range(1, SP):
-
-        @pl.when(sp + k < SP)
-        def _():
-            end_copy(k).start()
-
+    def send_ends(core):
+        for k in range(1, SP):
+
+            @pl.when(jnp.logical_and(core, sp + k < SP))
+            def _():
+                end_copy(k).start()
+
+    send_ends(first_core)
     pass_across(order[2])
 
-    def attend(qs, st, j, lo, hi, first=False, diagonal=False, qc=half, after=None):
+    def attend(qs, st, j, lo, hi, first=False, diagonal=False, qc=half, after=None, parts=None):
         ms, os = st
-        items = [(i, h) for i in range(rows // qc) for h in range(H)]
+        items = [(i, h) for i in (parts or range(rows // qc)) for h in range(H)]
 
         def width(i):
             return (lo, (i + 1) * qc) if diagonal else (lo, hi)
@@ -1261,45 +1289,62 @@
             part_out[r, h * HEAD_DIM : (h + 1) * HEAD_DIM] = o_far[h, r, 0:HEAD_DIM].astype(BF16)
             stats = jnp.where(lane == h, m_far[h, r, :], stats)
             stats = jnp.where(lane == H + h, o_far[h, r, HEAD_DIM:], stats)
-        stat_out[c] = stats.T[0:8, :]
-        for s in part_copies(c):
-            s.start()
+        stat_out[c] = stats.T[0 : 2 * H, :]
+        part, stat = part_copies(c)
+
+        @pl.when(first_core)
+        def _():
+            stat.start()
+
+        part.start()
+
+        @pl.when(jnp.logical_not(first_core))
+        def _():
+            stat.start()
 
     attend(q_ref, own_st, sp, 0, rows, True, True)
+
+    @pl.when(helper)
+    def _():
+        arrived(q_far.at[pl.ds(half, half)], qrecv.at[0])
+        attend(q_far, far_st, sp, 0, rows, True, parts=(1,))
 
     pass_up(order[3])
     pass_across(order[3])
-
+    send_ends(jnp.logical_not(first_core))
+
+    weight_pass(0, FAR)
     arrived(cum_buf.at[j_xo], crecv.at[ACROSS])
 
     @pl.when(helper)
     def _():
-        arrived(q_far, qrecv.at[0])
-        attend(q_far, far_st, sp, 0, rows, True)
+        arrived(q_far.at[pl.ds(0, half)], qrecv.at[1])
+        attend(q_far, far_st, sp, 0, rows, True, parts=(0,))
 
     for c in order:
         need = all_across(x == 1)
-        if c in via_z:
-            need = jnp.logical_and(need, jnp.logical_not(goes_up))
+        if c in climbs:
+            need = jnp.logical_and(need, jnp.logical_not(climbs[c]))
 
         @pl.when(need)
         def _():
             kv_wait(j_xo, c, ACROSS)
 
-    @pl.when(helper)
+    @pl.when(jnp.logical_and(helper, z == 0))
+    def _():
+        attend(q_far, far_st, j_xo, 0, rows, qc=rc, after=send_partial)
+
+    @pl.when(jnp.logical_and(helper, above0))
     def _():
         attend(q_far, far_st, j_xo, 0, rows)
 
-    @pl.when(jnp.logical_and(helper, z == 0))
-    def _():
-        for c in range(CH):
-            send_partial(c)
+    weight_pass(0, PFAR)
 
     @pl.when(above0)
     def _():
-        for c in via_z:
-
-            @pl.when(jnp.logical_not(all_over_x))
+        for c in climbs:
+
+            @pl.when(jnp.logical_not(crosses.get(c, False)))
             def _():
                 kv_wait(j_b, c, BELOW)
 
@@ -1310,16 +1355,21 @@
     def _():
         attend(q_far, far_st, j_b, 0, rows)
 
-    weight_pass(0, FAR)
-    weight_pass(0, PFAR)
+    @pl.when(above0)
+    def _():
+        attend(q_ref, own_st, j_b, 0, rows)
+
+    weight_pass(1, FAR)
+
+    @pl.when(jnp.logical_and(helper, above0))
+    def _():
+        for c in order[0:2]:
+            kv_wait(j_bo, c, DIAG)
+        attend(q_far, far_st, j_bo, half, rows)
 
     @pl.when(x == 1)
     def _():
         attend(q_ref, own_st, j_xo, 0, rows)
-
-    @pl.when(above0)
-    def _():
-        attend(q_ref, own_st, j_b, 0, rows)
 
     carry_ref[0:1, :] = jnp.zeros((1, lw), F32)
     for j in range(SP - 1):
@@ -1343,29 +1393,30 @@
     own_lru = br_lru.at[tp]
     send(own_lru, lsend.at[0], lrecv.at[FAR], {"tp": far})
     send(own_lru, lsend.at[0], lrecv.at[PARTNER], {"tp": partner})
-    weight_pass(1, FAR)
-
-    @pl.when(above0)
+    weight_pass(1, PFAR)
+
+    upper = jnp.logical_and(above0, jnp.logical_not(helper))
+    middle = jnp.logical_and(above0, helper)
+
+    @pl.when(upper)
     def _():
         for c in order[0:2]:
             kv_wait(j_bo, c, DIAG)
-
-        @pl.when(helper)
-        def _():
-            attend(q_far, far_st, j_bo, half, rows)
-
+        attend(q_ref, own_st, j_bo, half, rows)
+
+    @pl.when(above0)
+    def _():
         for c in order[2:]:
             kv_wait(j_bo, c, DIAG)
 
-        @pl.when(helper)
-        def _():
-            attend(q_far, far_st, j_bo, 0, half, qc=rc, after=send_partial)
-
-    weight_pass(1, PFAR)
-
-    @pl.when(above0)
-    def _():
+    @pl.when(middle)
+    def _():
+        attend(q_far, far_st, j_bo, 0, half, qc=rc, after=send_partial)
         attend(q_ref, own_st, j_bo, 0, rows)
+
+    @pl.when(upper)
+    def _():
+        attend(q_ref, own_st, j_bo, 0, half)
 
     def pair_dot(br, buf, side, r):
         first = 2 * side
@@ -1373,14 +1424,6 @@
             br[first + 1, r, :], buf[first + 1], preferred_element_type=F32
         )
 
-    for c in own_loads:
-        c.wait()
-    for n in range(2):
-        arrived(banks[n][1].at[partner], wrecv_own.at[n])
-    arrived(br_lru.at[partner], lrecv.at[PARTNER])
-    for c in range(CH):
-        oacc[chunk(c), :] = pair_dot(br_lru, wl_buf, y, chunk(c))
-
     for c in range(CH):
         r = slice(c * rc, (c + 1) * rc)
 
@@ -1388,7 +1431,7 @@
         def _():
             for s in part_copies(c):
                 s.wait_recv()
-            stats = jnp.concatenate([stat_in[c], jnp.zeros((120, rc), F32)], axis=0).T
+            stats = jnp.concatenate([stat_in[c], jnp.zeros((128 - 2 * H, rc), F32)], axis=0).T
             for h in range(H):
                 hs = slice(h * HEAD_DIM, (h + 1) * HEAD_DIM)
                 m_in = stats[:, h : h + 1]
@@ -1413,6 +1456,16 @@
         send(ref, fsend.at[0], frecv.at[FAR, c], {"tp": far})
         send(ref, fsend.at[1], frecv.at[PARTNER, c], {"tp": partner})
 
+    weight_pass_bottom(FAR)
+    weight_pass_bottom(PFAR)
+    for c in own_loads:
+        c.wait()
+    for n in range(2):
+        arrived(banks[n][1].at[partner], wrecv_own.at[n])
+    arrived(br_lru.at[partner], lrecv.at[PARTNER])
+    for c in range(CH):
+        oacc[chunk(c), :] = pair_dot(br_lru, wl_buf, y, chunk(c))
+
     arrived(br_lru.at[far], lrecv.at[FAR])
     send(br_lru.at[far], lsend.at[1], lrecv.at[PFAR], {"tp": partner})
     for role in (FAR, PFAR):
@@ -1444,13 +1497,21 @@
         sent(br_fox.at[0], fsend.at[k])
     sent(br_lru.at[pl.ds(0, 2)], lsend.at[0])
     sent(br_lru.at[0], lsend.at[1])
-    for k in range(2):
-        sent(wl_buf.at[pl.ds(0, 2)], wsend.at[k])
-
-    @pl.when(odd)
-    def _():
-        for k in range(2, 4):
-            sent(wl_buf.at[pl.ds(0, 2)], wsend.at[k])
+    sent(wl_buf.at[0], wsend.at[1])
+    sent(wl_buf.at[pl.ds(0, 2)], wsend.at[2])
+
+    @pl.when(above0)
+    def _():
+        sent(wl_buf.at[0], wsend.at[0])
+        sent(wl_buf.at[pl.ds(0, 2)], wsend.at[3])
+
+    @pl.when(top)
+    def _():
+        sent(wl_buf.at[pl.ds(0, 2)], wsend.at[4])
+
+    @pl.when(z == 0)
+    def _():
+        sent(wl_buf.at[0], wsend.at[4])
 
     sent(own_cum, csend.at[0])
     top_half = pl.ds(0, half)
@@ -1460,21 +1521,20 @@
     def _():
         sent(kv_buf.at[0], xsend.at[0])
 
-    @pl.when(jnp.logical_and(goes_up, jnp.logical_not(need)))
+    @pl.when(jnp.logical_and(second_top, jnp.logical_not(need)))
     def _():
         sent(kv_buf.at[0, top_half], xsend.at[0])
 
-    @pl.when(goes_up)
-    def _():
-        sent(kv_buf.at[0, top_half], zfwd.at[0])
-
-    @pl.when(all_over_x)
-    def _():
-        sent(kv_buf.at[0], xfwd.at[0])
-
-    @pl.when(jnp.logical_and(above0, jnp.logical_not(all_over_x)))
-    def _():
-        sent(kv_buf.at[0, top_half], xfwd.at[0])
+    for level in range(Z):
+
+        @pl.when(z == level)
+        def _():
+            ups = (level < Z - 1) + (level == Z - 2)
+            if ups:
+                sent(kv_buf.at[0, pl.ds(0, ups * rc)], zfwd.at[0])
+            overs = (2 if level else 0) + (0 < level < Z - 1)
+            if overs:
+                sent(kv_buf.at[0, pl.ds(0, overs * rc)], xfwd.at[0])
 
     @pl.when(not_top)
     def _():
@@ -1539,18 +1599,18 @@
         V((8, lw), F32),
         V((8, lw), F32),
         V((8, lw), F32),
-        V((SP, 8, lw), F32),
+        V((SP, 2, lw), F32),
         V((SP, rows, 2 * fw), BF16),
-        V((SP, 8, rows), F32),
+        V((SP, H, rows), F32),
         V((H, rows, 128), F32),
         V((H, rows, 2 * HEAD_DIM), F32),
         V((rows, fw), BF16),
         V((H, rows, 128), F32),
         V((H, rows, 2 * HEAD_DIM), F32),
         V((rows, fw), BF16),
-        V((CH, 8, rc), F32),
+        V((CH, 2 * H, rc), F32),
         V((rows, fw), BF16),
-        V((CH, 8, rc), F32),
+        V((CH, 2 * H, rc), F32),
         V((TP, lw, oc), BF16),
         V((TP, fw, oc), BF16),
         V((TP, rows, lw), BF16),
@@ -1570,7 +1630,7 @@
         dma((1,)),
         dma((1,)),
         dma((3, CH)),
-        dma((4,)),
+        dma((5,)),
         dma((2,)),
         dma((2, 2, X)),
         dma((2,)),
@@ -1578,7 +1638,7 @@
         dma((3,)),
         dma((3, CH)),
         dma((1,)),
-        dma((1,)),
+        dma((2,)),
         dma((2,)),
         dma((CH, 2)),
     ]

time: 50 us -> 47.5 us (0.950)
  Pallas kernels: 49 us -> 46.3 us
    pallas_call x1, Pallas kernels: 49 us -> 46.3 us  [block_shards(): pl.pallas_call(functools.partial(block_kernel, SP, TP, X, CH), out_shape=...]
where the time goes in v3:
time: 47.5 us; the launch traced here: 47.1 us
  Pallas kernels  46.3 us (97%)
  local copies, waits for them, and re-layouts  0.8 us (2%)
    pallas_call x1, Pallas kernels, block_shards(): pl.pallas_call(functools.partial(block_kernel, SP, TP, X, CH), out_shape=...  46.3 us

profile of v3, /device:TPU:25, one launch (start us, length us, event | category | flops | bytes accessed | tf_op | source)
XLA Modules:
  0.0 47.1 jit_solution(2560153221980903419)
XLA Ops:
  0.0 46.3 %shard_map.136 = bf16[512,512]{1,0:T(8,128)(2,1)S(1)} custom-call(bf16[512,512]{1,0:T(8,128)(2,1)} %tokens.1, bf16[2048,256]{1,0:T(8,128)(2,1)} %lru_in.1, bf16[2048,256]{1,0:T(8,128)(2,1)} %gate_in.1, bf16[2048,256]{1,0:T(8,128)(2,1)} %query_w.1, bf16[2048,256]{1,0:T(8,128)(2,1)} %key_w.1, bf16[2048,256]{1,0:T(8,128)(2,1)} %value_w.1, ...), custom_call_target="tpu_custom_call" | custom-call | tf_op jit(solution)/shard_map/pallas_call | solution.py:1645
  46.3 0.8 %copy.16 = bf16[512,512]{1,0:T(8,128)(2,1)} copy(bf16[512,512]{1,0:T(8,128)(2,1)S(1)} %shard_map.136) | data formatting | bytes 1048576

commit v4 on v3

--- a/solution.py
+++ b/solution.py
@@ -893,13 +893,22 @@
     }
     whalf = lax.rem(x + z, X)
     top = z == Z - 1
-    first_core = lax.rem(tp, 2) == 0
     PARTNER, FAR, PFAR = 0, 1, 2
     ACROSS, BELOW, DIAG = 0, 1, 2
     score_k = HEAD_DIM ** (-0.5) * LOG2E
 
     def chunk(c):
         return pl.ds(c * rc, rc)
+
+    pieces = [(c * rc, rc) for c in range(CH - 1)]
+    pieces += [(rows - rc, rc // 2), (rows - rc // 2, rc // 2)]
+    PC = len(pieces)
+
+    def piece(k):
+        return pl.ds(*pieces[k])
+
+    def pieces_of(c):
+        return [k for k, (at, n) in enumerate(pieces) if at // rc == c]
 
     barrier = pltpu.get_barrier_semaphore()
     for k in range(1, SP):
@@ -1203,19 +1212,14 @@
         return remote(
             ends.at[sp],
             ends.at[sp],
-            esend.at[k - 1],
-            erecv.at[lax.rem(sp, SP - 1)],
+            esend.at[0],
+            erecv.at[0],
             {"sp": lax.rem(sp + k, SP)},
         )
 
-    def send_ends(core):
-        for k in range(1, SP):
-
-            @pl.when(jnp.logical_and(core, sp + k < SP))
-            def _():
-                end_copy(k).start()
-
-    send_ends(first_core)
+    for k in range(1, SP):
+        end_copy(k).start()
+
     pass_across(order[2])
 
     def attend(qs, st, j, lo, hi, first=False, diagonal=False, qc=half, after=None, parts=None):
@@ -1275,11 +1279,12 @@
     far_st = (m_far, o_far)
     up2 = {"sp": lax.rem(sp + 2 * X, SP)}
 
-    def part_copies(c):
-        return (
-            remote(part_out.at[chunk(c)], part_in.at[chunk(c)], osend.at[0], orecv.at[c, 0], up2),
-            remote(stat_out.at[c], stat_in.at[c], osend.at[1], orecv.at[c, 1], up2),
-        )
+    def part_copy(k):
+        r = piece(k)
+        return remote(part_out.at[r], part_in.at[r], osend.at[0], orecv.at[k], up2)
+
+    def stat_copy(c):
+        return remote(stat_out.at[c], stat_in.at[c], osend.at[1], orecv.at[PC + c], up2)
 
     def send_partial(c):
         r = slice(c * rc, (c + 1) * rc)
@@ -1290,17 +1295,9 @@
             stats = jnp.where(lane == h, m_far[h, r, :], stats)
             stats = jnp.where(lane == H + h, o_far[h, r, HEAD_DIM:], stats)
         stat_out[c] = stats.T[0 : 2 * H, :]
-        part, stat = part_copies(c)
-
-        @pl.when(first_core)
-        def _():
-            stat.start()
-
-        part.start()
-
-        @pl.when(jnp.logical_not(first_core))
-        def _():
-            stat.start()
+        stat_copy(c).start()
+        for k in pieces_of(c):
+            part_copy(k).start()
 
     attend(q_ref, own_st, sp, 0, rows, True, True)
 
@@ -1311,15 +1308,9 @@
 
     pass_up(order[3])
     pass_across(order[3])
-    send_ends(jnp.logical_not(first_core))
 
     weight_pass(0, FAR)
     arrived(cum_buf.at[j_xo], crecv.at[ACROSS])
-
-    @pl.when(helper)
-    def _():
-        arrived(q_far.at[pl.ds(0, half)], qrecv.at[1])
-        attend(q_far, far_st, sp, 0, rows, True, parts=(0,))
 
     for c in order:
         need = all_across(x == 1)
@@ -1330,12 +1321,21 @@
         def _():
             kv_wait(j_xo, c, ACROSS)
 
-    @pl.when(jnp.logical_and(helper, z == 0))
-    def _():
-        attend(q_far, far_st, j_xo, 0, rows, qc=rc, after=send_partial)
-
-    @pl.when(jnp.logical_and(helper, above0))
-    def _():
+    @pl.when(z == 0)
+    def _():
+        late = range(CH // 2, CH)
+        attend(q_far, far_st, j_xo, 0, rows, qc=rc, after=send_partial, parts=late)
+        arrived(q_far.at[pl.ds(0, half)], qrecv.at[1])
+        attend(q_far, far_st, sp, 0, rows, True, parts=(0,))
+        early = range(CH // 2)
+        attend(q_far, far_st, j_xo, 0, rows, qc=rc, after=send_partial, parts=early)
+
+    middle = jnp.logical_and(above0, helper)
+
+    @pl.when(middle)
+    def _():
+        arrived(q_far.at[pl.ds(0, half)], qrecv.at[1])
+        attend(q_far, far_st, sp, 0, rows, True, parts=(0,))
         attend(q_far, far_st, j_xo, 0, rows)
 
     weight_pass(0, PFAR)
@@ -1351,7 +1351,7 @@
         arrived(cum_buf.at[j_b], crecv.at[BELOW])
         arrived(cum_buf.at[j_bo], crecv.at[DIAG])
 
-    @pl.when(jnp.logical_and(helper, above0))
+    @pl.when(middle)
     def _():
         attend(q_far, far_st, j_b, 0, rows)
 
@@ -1359,24 +1359,13 @@
     def _():
         attend(q_ref, own_st, j_b, 0, rows)
 
-    weight_pass(1, FAR)
-
-    @pl.when(jnp.logical_and(helper, above0))
-    def _():
-        for c in order[0:2]:
-            kv_wait(j_bo, c, DIAG)
-        attend(q_far, far_st, j_bo, half, rows)
-
-    @pl.when(x == 1)
-    def _():
-        attend(q_ref, own_st, j_xo, 0, rows)
-
     carry_ref[0:1, :] = jnp.zeros((1, lw), F32)
+    others = ends.at[pl.ds(0, SP - 1)]
+    arrived(others, erecv.at[0])
     for j in range(SP - 1):
 
         @pl.when(j < sp)
         def _():
-            arrived(ends.at[j], erecv.at[j])
             carry_ref[0:1, :] = ends[j, 0:1, :] * carry_ref[0:1, :] + ends[j, 1:2, :]
 
     carry = carry_ref[0:1, :]
@@ -1393,30 +1382,62 @@
     own_lru = br_lru.at[tp]
     send(own_lru, lsend.at[0], lrecv.at[FAR], {"tp": far})
     send(own_lru, lsend.at[0], lrecv.at[PARTNER], {"tp": partner})
-    weight_pass(1, PFAR)
-
-    upper = jnp.logical_and(above0, jnp.logical_not(helper))
-    middle = jnp.logical_and(above0, helper)
-
-    @pl.when(upper)
+    weight_pass(1, FAR)
+
+    @pl.when(jnp.logical_and(helper, above0))
     def _():
         for c in order[0:2]:
             kv_wait(j_bo, c, DIAG)
-        attend(q_ref, own_st, j_bo, half, rows)
-
-    @pl.when(above0)
-    def _():
-        for c in order[2:]:
-            kv_wait(j_bo, c, DIAG)
-
-    @pl.when(middle)
-    def _():
-        attend(q_far, far_st, j_bo, 0, half, qc=rc, after=send_partial)
-        attend(q_ref, own_st, j_bo, 0, rows)
-
-    @pl.when(upper)
-    def _():
-        attend(q_ref, own_st, j_bo, 0, half)
+        attend(q_far, far_st, j_bo, half, rows)
+
+    @pl.when(x == 1)
+    def _():
+        attend(q_ref, own_st, j_xo, 0, rows)
+
+    weight_pass(1, PFAR)
+
+    upper = jnp.logical_and(above0, jnp.logical_not(helper))
+
+    def heads_of(h):
+        return slice(h * HEAD_DIM, (h + 1) * HEAD_DIM)
+
+    def send_fox(k):
+        ref = br_fox.at[tp, piece(k)]
+        send(ref, fsend.at[0], frecv.at[FAR, k], {"tp": far})
+        send(ref, fsend.at[1], frecv.at[PARTNER, k], {"tp": partner})
+
+    def finish_rows(c):
+        r = slice(c * rc, (c + 1) * rc)
+        for h in range(H):
+            br_fox[tp, r, heads_of(h)] = (o_ref[h, r, 0:HEAD_DIM] / o_ref[h, r, HEAD_DIM:]).astype(
+                BF16
+            )
+        for k in pieces_of(c):
+            send_fox(k)
+
+    def merge_rows(c):
+        for k in pieces_of(c):
+            at, n = pieces[k]
+            arrived(part_in.at[piece(k)], orecv.at[k])
+            if k == pieces_of(c)[0]:
+                arrived(stat_in.at[c], orecv.at[PC + c])
+                pad_rows = jnp.zeros((128 - 2 * H, rc), F32)
+                stats = jnp.concatenate([stat_in[c], pad_rows], axis=0).T
+            r = slice(at, at + n)
+            mine = slice(at - c * rc, at - c * rc + n)
+            for h in range(H):
+                m_in = stats[mine, h : h + 1]
+                l_in = stats[mine, H + h : H + h + 1]
+                part = part_in[r, heads_of(h)].astype(F32)
+                old = m_ref[h, r, :]
+                new = jnp.maximum(old, m_in)
+                fade = jnp.exp2(old - new)
+                grow = jnp.exp2(m_in - new)
+                total = o_ref[h, r, HEAD_DIM:] * fade + l_in * grow
+                br_fox[tp, r, heads_of(h)] = (
+                    (o_ref[h, r, 0:HEAD_DIM] * fade + part * grow) / total
+                ).astype(BF16)
+            send_fox(k)
 
     def pair_dot(br, buf, side, r):
         first = 2 * side
@@ -1424,72 +1445,90 @@
             br[first + 1, r, :], buf[first + 1], preferred_element_type=F32
         )
 
-    for c in range(CH):
-        r = slice(c * rc, (c + 1) * rc)
-
-        @pl.when(helped)
-        def _():
-            for s in part_copies(c):
-                s.wait_recv()
-            stats = jnp.concatenate([stat_in[c], jnp.zeros((128 - 2 * H, rc), F32)], axis=0).T
-            for h in range(H):
-                hs = slice(h * HEAD_DIM, (h + 1) * HEAD_DIM)
-                m_in = stats[:, h : h + 1]
-                l_in = stats[:, H + h : H + h + 1]
-                part = part_in[r, hs].astype(F32)
-                old = m_ref[h, r, :]
-                new = jnp.maximum(old, m_in)
-                fade = jnp.exp2(old - new)
-                grow = jnp.exp2(m_in - new)
-                total = o_ref[h, r, HEAD_DIM:] * fade + l_in * grow
-                br_fox[tp, r, hs] = (
-                    (o_ref[h, r, 0:HEAD_DIM] * fade + part * grow) / total
-                ).astype(BF16)
-
-        @pl.when(jnp.logical_not(helped))
-        def _():
-            for h in range(H):
-                hs = slice(h * HEAD_DIM, (h + 1) * HEAD_DIM)
-                br_fox[tp, r, hs] = (o_ref[h, r, 0:HEAD_DIM] / o_ref[h, r, HEAD_DIM:]).astype(BF16)
-
-        ref = br_fox.at[tp, chunk(c)]
-        send(ref, fsend.at[0], frecv.at[FAR, c], {"tp": far})
-        send(ref, fsend.at[1], frecv.at[PARTNER, c], {"tp": partner})
+    def lru_near():
+        for c in own_loads:
+            c.wait()
+        for n in range(2):
+            arrived(banks[n][1].at[partner], wrecv_own.at[n])
+        arrived(br_lru.at[partner], lrecv.at[PARTNER])
+        for c in range(CH):
+            oacc[chunk(c), :] = pair_dot(br_lru, wl_buf, y, chunk(c))
+
+    def lru_relay():
+        arrived(br_lru.at[far], lrecv.at[FAR])
+        send(br_lru.at[far], lsend.at[1], lrecv.at[PFAR], {"tp": partner})
+
+    def lru_far():
+        for role in (FAR, PFAR):
+            weight_wait(0, role)
+        arrived(br_lru.at[pfar], lrecv.at[PFAR])
+        for c in range(CH):
+            oacc[chunk(c), :] += pair_dot(br_lru, wl_buf, 1 - y, chunk(c))
+
+    @pl.when(upper)
+    def _():
+        for c in order[0:2]:
+            kv_wait(j_bo, c, DIAG)
+        attend(q_ref, own_st, j_bo, half, rows)
+
+    @pl.when(above0)
+    def _():
+        for c in order[2:]:
+            kv_wait(j_bo, c, DIAG)
+
+    @pl.when(middle)
+    def _():
+        attend(q_far, far_st, j_bo, 0, half, qc=rc, after=send_partial)
+        attend(q_ref, own_st, j_bo, 0, rows, qc=rc, after=finish_rows)
+
+    @pl.when(upper)
+    def _():
+        attend(q_ref, own_st, j_bo, 0, half)
+
+    @pl.when(top)
+    def _():
+        lru_near()
+        merge_rows(0)
+        merge_rows(1)
+        lru_relay()
+        merge_rows(2)
+        lru_far()
+        merge_rows(3)
+
+    @pl.when(second_top)
+    def _():
+        for c in range(CH):
+            merge_rows(c)
+
+    @pl.when(z == 0)
+    def _():
+        for c in range(CH):
+            finish_rows(c)
 
     weight_pass_bottom(FAR)
     weight_pass_bottom(PFAR)
-    for c in own_loads:
-        c.wait()
-    for n in range(2):
-        arrived(banks[n][1].at[partner], wrecv_own.at[n])
-    arrived(br_lru.at[partner], lrecv.at[PARTNER])
-    for c in range(CH):
-        oacc[chunk(c), :] = pair_dot(br_lru, wl_buf, y, chunk(c))
-
-    arrived(br_lru.at[far], lrecv.at[FAR])
-    send(br_lru.at[far], lsend.at[1], lrecv.at[PFAR], {"tp": partner})
+
+    @pl.when(not_top)
+    def _():
+        lru_near()
+        lru_relay()
+        lru_far()
+
     for role in (FAR, PFAR):
-        weight_wait(0, role)
         weight_wait(1, role)
-    arrived(br_lru.at[pfar], lrecv.at[PFAR])
-    for c in range(CH):
-        oacc[chunk(c), :] += pair_dot(br_lru, wl_buf, 1 - y, chunk(c))
-
-    def fox_wait(src, role, c):
-        arrived(br_fox.at[src, chunk(c)], frecv.at[role, c])
-
-    def fox_pass(c):
-        fox_wait(far, FAR, c)
-        send(br_fox.at[far, chunk(c)], fsend.at[2], frecv.at[PFAR, c], {"tp": partner})
+
+    def fox_pass(k):
+        arrived(br_fox.at[far, piece(k)], frecv.at[FAR, k])
+        send(br_fox.at[far, piece(k)], fsend.at[2], frecv.at[PFAR, k], {"tp": partner})
 
     fox_pass(0)
-    for c in range(CH):
-        r = chunk(c)
-        if c + 1 < CH:
-            fox_pass(c + 1)
-        fox_wait(partner, PARTNER, c)
+    for k in range(PC):
+        r = piece(k)
+        if k + 1 < PC:
+            fox_pass(k + 1)
+        arrived(br_fox.at[partner, r], frecv.at[PARTNER, k])
         oacc[r, :] += pair_dot(br_fox, wf_buf, y, r)
-        fox_wait(pfar, PFAR, c)
+        arrived(br_fox.at[pfar, r], frecv.at[PFAR, k])
         out[r, :] = (oacc[r, :] + pair_dot(br_fox, wf_buf, 1 - y, r)).astype(out.dtype)
 
     for k in range(3):
@@ -1554,11 +1593,7 @@
     def _():
         halo_copy.wait_send()
 
-    for k in range(1, SP):
-
-        @pl.when(sp + k < SP)
-        def _():
-            end_copy(k).wait_send()
+    sent(others, esend.at[0])
 
 
 def block_shards(SP, TP, X, *args):
@@ -1621,8 +1656,8 @@
         dma((3, CH)),
         dma((1,)),
         dma((1,)),
-        dma((SP - 1,)),
-        dma((SP - 1,)),
+        dma((1,)),
+        dma((1,)),
         dma((2,)),
         dma((3,)),
         dma((1,)),
@@ -1636,11 +1671,11 @@
         dma((2,)),
         dma((3,)),
         dma((3,)),
-        dma((3, CH)),
+        dma((3, CH + 1)),
         dma((1,)),
         dma((2,)),
         dma((2,)),
-        dma((CH, 2)),
+        dma((2 * CH + 1,)),
     ]
     return pl.pallas_call(
         functools.partial(block_kernel, SP, TP, X, CH),

time: 47.5 us -> 46.8 us (0.985)
  no operation moved by 1% of the time
where the time goes in v4:
time: 46.8 us; the launch traced here: 46.7 us
  Pallas kernels  45.9 us (98%)
  local copies, waits for them, and re-layouts  0.8 us (2%)
    pallas_call x1, Pallas kernels, block_shards(): pl.pallas_call(functools.partial(block_kernel, SP, TP, X, CH), out_shape=...  45.9 us

profile of v4, /device:TPU:25, one launch (start us, length us, event | category | flops | bytes accessed | tf_op | source)
XLA Modules:
  0.0 46.7 jit_solution(18352832381857183259)
XLA Ops:
  0.0 45.9 %shard_map.136 = bf16[512,512]{1,0:T(8,128)(2,1)S(1)} custom-call(bf16[512,512]{1,0:T(8,128)(2,1)} %tokens.1, bf16[2048,256]{1,0:T(8,128)(2,1)} %lru_in.1, bf16[2048,256]{1,0:T(8,128)(2,1)} %gate_in.1, bf16[2048,256]{1,0:T(8,128)(2,1)} %query_w.1, bf16[2048,256]{1,0:T(8,128)(2,1)} %key_w.1, bf16[2048,256]{1,0:T(8,128)(2,1)} %value_w.1, ...), custom_call_target="tpu_custom_call" | custom-call | tf_op jit(solution)/shard_map/pallas_call | solution.py:1680
  45.9 0.8 %copy.16 = bf16[512,512]{1,0:T(8,128)(2,1)} copy(bf16[512,512]{1,0:T(8,128)(2,1)S(1)} %shard_map.136) | data formatting | bytes 1048576

commit v5 on v4

--- a/solution.py
+++ b/solution.py
@@ -885,12 +885,11 @@
     above0 = z >= 1
     order = list(range(CH - 1, -1, -1))
     second_top = z == Z - 2
-    climbs = {order[1]: not_top, order[3]: second_top}
-    crosses = {
-        order[0]: above0,
-        order[2]: above0,
-        order[3]: jnp.logical_and(above0, not_top),
-    }
+    last = order[3]
+    last_climbs = jnp.logical_and(not_top, z != Z - 3)
+    last_crosses = jnp.logical_and(above0, not_top)
+    climbs = {order[1]: not_top, last: last_climbs}
+    crosses = {order[0]: above0, order[2]: above0, last: last_crosses}
     whalf = lax.rem(x + z, X)
     top = z == Z - 1
     PARTNER, FAR, PFAR = 0, 1, 2
@@ -1142,6 +1141,42 @@
         def _():
             kv_wait(j_b, c, BELOW)
             kv_send(j_b, c, xfwd, DIAG, to_xo)
+
+    cut = rc - rc // 4
+
+    def half_ref(j, upper_part):
+        at, n = (cut, rc - cut) if upper_part else (0, cut)
+        return kv_buf.at[j, pl.ds(last * rc + at, n)]
+
+    def half_sem(upper_part):
+        return kvrecv.at[DIAG, last] if upper_part else kvrecv.at[DIAG, CH]
+
+    def pass_up_last():
+        @pl.when(last_climbs)
+        def _():
+            kv_wait(j_xo, last, ACROSS)
+            send(half_ref(j_xo, True), zfwd.at[0], half_sem(True), to_up)
+
+        @pl.when(second_top)
+        def _():
+            send(half_ref(j_xo, False), zfwd.at[0], half_sem(False), to_up)
+
+    def pass_across_last():
+        @pl.when(last_crosses)
+        def _():
+            kv_wait(j_b, last, BELOW)
+            send(half_ref(j_b, False), xfwd.at[0], half_sem(False), to_xo)
+
+        @pl.when(second_top)
+        def _():
+            send(half_ref(j_b, True), xfwd.at[0], half_sem(True), to_xo)
+
+    def diag_wait(c):
+        if c == last:
+            for upper_part in (True, False):
+                arrived(half_ref(j_bo, upper_part), half_sem(upper_part))
+        else:
+            kv_wait(j_bo, c, DIAG)
 
     near_part(order[0], 0)
     for i, c in enumerate(order):
@@ -1306,8 +1341,8 @@
         arrived(q_far.at[pl.ds(half, half)], qrecv.at[0])
         attend(q_far, far_st, sp, 0, rows, True, parts=(1,))
 
-    pass_up(order[3])
-    pass_across(order[3])
+    pass_up_last()
+    pass_across_last()
 
     weight_pass(0, FAR)
     arrived(cum_buf.at[j_xo], crecv.at[ACROSS])
@@ -1387,7 +1422,7 @@
     @pl.when(jnp.logical_and(helper, above0))
     def _():
         for c in order[0:2]:
-            kv_wait(j_bo, c, DIAG)
+            diag_wait(c)
         attend(q_far, far_st, j_bo, half, rows)
 
     @pl.when(x == 1)
@@ -1404,6 +1439,8 @@
     def send_fox(k):
         ref = br_fox.at[tp, piece(k)]
         send(ref, fsend.at[0], frecv.at[FAR, k], {"tp": far})
+        if k == PC - 1:
+            send(ref, fsend.at[2], frecv.at[PFAR, k], {"tp": pfar})
         send(ref, fsend.at[1], frecv.at[PARTNER, k], {"tp": partner})
 
     def finish_rows(c):
@@ -1468,13 +1505,13 @@
     @pl.when(upper)
     def _():
         for c in order[0:2]:
-            kv_wait(j_bo, c, DIAG)
+            diag_wait(c)
         attend(q_ref, own_st, j_bo, half, rows)
 
     @pl.when(above0)
     def _():
         for c in order[2:]:
-            kv_wait(j_bo, c, DIAG)
+            diag_wait(c)
 
     @pl.when(middle)
     def _():
@@ -1519,7 +1556,8 @@
 
     def fox_pass(k):
         arrived(br_fox.at[far, piece(k)], frecv.at[FAR, k])
-        send(br_fox.at[far, piece(k)], fsend.at[2], frecv.at[PFAR, k], {"tp": partner})
+        if k < PC - 1:
+            send(br_fox.at[far, piece(k)], fsend.at[2], frecv.at[PFAR, k], {"tp": partner})
 
     fox_pass(0)
     for k in range(PC):
@@ -1568,12 +1606,14 @@
 
         @pl.when(z == level)
         def _():
-            ups = (level < Z - 1) + (level == Z - 2)
+            ups = (level < Z - 1) * rc + (level < Z - 1 and level != Z - 3) * (rc - cut)
+            ups += (level == Z - 2) * cut
             if ups:
-                sent(kv_buf.at[0, pl.ds(0, ups * rc)], zfwd.at[0])
-            overs = (2 if level else 0) + (0 < level < Z - 1)
+                sent(kv_buf.at[0, pl.ds(0, ups)], zfwd.at[0])
+            overs = (2 * rc if level else 0) + (level == Z - 2) * (rc - cut)
+            overs += (0 < level < Z - 1) * cut
             if overs:
-                sent(kv_buf.at[0, pl.ds(0, overs * rc)], xfwd.at[0])
+                sent(kv_buf.at[0, pl.ds(0, overs)], xfwd.at[0])
 
     @pl.when(not_top)
     def _():
@@ -1664,7 +1704,7 @@
         dma((1,)),
         dma((1,)),
         dma((1,)),
-        dma((3, CH)),
+        dma((3, CH + 1)),
         dma((5,)),
         dma((2,)),
         dma((2, 2, X)),

time: 46.8 us -> 46.4 us (level)
  Pallas kernels: 45.9 us -> 45 us
    pallas_call x1, Pallas kernels: 45.9 us -> 45 us  [block_shards(): pl.pallas_call(functools.partial(block_kernel, SP, TP, X, CH), out_shape=...]
where the time goes in v5:
time: 46.4 us; the launch traced here: 45.8 us
  Pallas kernels  45 us (97%)
  local copies, waits for them, and re-layouts  0.8 us (2%)
    pallas_call x1, Pallas kernels, block_shards(): pl.pallas_call(functools.partial(block_kernel, SP, TP, X, CH), out_shape=...  45 us

profile of v5, /device:TPU:25, one launch (start us, length us, event | category | flops | bytes accessed | tf_op | source)
XLA Modules:
  0.0 45.8 jit_solution(1324489752745019790)
XLA Ops:
  0.0 45.0 %shard_map.136 = bf16[512,512]{1,0:T(8,128)(2,1)S(1)} custom-call(bf16[512,512]{1,0:T(8,128)(2,1)} %tokens.1, bf16[2048,256]{1,0:T(8,128)(2,1)} %lru_in.1, bf16[2048,256]{1,0:T(8,128)(2,1)} %gate_in.1, bf16[2048,256]{1,0:T(8,128)(2,1)} %query_w.1, bf16[2048,256]{1,0:T(8,128)(2,1)} %key_w.1, bf16[2048,256]{1,0:T(8,128)(2,1)} %value_w.1, ...), custom_call_target="tpu_custom_call" | custom-call | tf_op jit(solution)/shard_map/pallas_call | solution.py:1720
  45.0 0.8 %copy.16 = bf16[512,512]{1,0:T(8,128)(2,1)} copy(bf16[512,512]{1,0:T(8,128)(2,1)S(1)} %shard_map.136) | data formatting | bytes 1048576

commit v6 on v5

--- a/solution.py
+++ b/solution.py
@@ -832,6 +832,7 @@
     oacc,
     load_sem,
     tsend,
+    trecv_near,
     trecv,
     hsend,
     hrecv,
@@ -850,6 +851,7 @@
     lsend,
     lrecv,
     fsend,
+    frecv_near,
     frecv,
     qsend,
     qrecv,
@@ -924,28 +926,25 @@
         c.start()
         return c
 
-    tok_loads = [
-        load(n, tokens.at[chunk(c)], tok_buf.at[tp, chunk(c)]) for n, c in enumerate(order)
-    ]
+    for c in order:
+        load(0, tokens.at[chunk(c)], tok_buf.at[tp, chunk(c)])
     cols = (0, fw, 2 * fw, 2 * fw + lw, 3 * fw + lw, 3 * fw + 2 * lw)
     for i, w in enumerate((key_w, value_w, lru_in, query_w, gate_in)):
-        load(CH, w, w_buf.at[:, cols[i] : cols[i + 1]])
+        load(1, w, w_buf.at[:, cols[i] : cols[i + 1]])
     mine = pl.ds(pl.multiple_of(tp * oc, 128), oc)
     bw = rg_w.shape[1]
     nb = lw // bw
     gates = pl.ds(tp * nb, nb)
-    forget_load = load(CH + 1, forget, forget_v)
+    forget_load = load(2, forget, forget_v)
     small_loads = [
-        load(CH + 2, conv_w, conv_v),
-        load(CH + 3, rg_w.at[gates], rg_v),
-        load(CH + 4, ig_w.at[gates], ig_v),
-        load(CH + 5, rate, rate_v),
-        load(CH + 6, decay_extra, decay_buf),
+        load(3, conv_w, conv_v),
+        load(4, rg_w.at[gates], rg_v),
+        load(5, ig_w.at[gates], ig_v),
+        load(6, rate, rate_v),
+        load(7, decay_extra, decay_buf),
     ]
-    own_loads = [
-        load(CH + 7, out_lru.at[:, mine], wl_buf.at[tp]),
-        load(CH + 8, out_fox.at[:, mine], wf_buf.at[tp]),
-    ]
+    load(8, out_lru.at[:, mine], wl_buf.at[tp])
+    load(8, out_fox.at[:, mine], wf_buf.at[tp])
     pl.semaphore_wait(barrier, SP - 1 + TP - 1)
 
     def send(ref, send_sem, recv_sem, device):
@@ -957,12 +956,14 @@
     def sent(ref, send_sem):
         remote(ref, ref, send_sem, send_sem, to_xo).wait_send()
 
-    for n, c in enumerate(order):
-        tok_loads[n].wait()
+    own_rows = tok_buf.at[tp]
+    pltpu.make_async_copy(own_rows, own_rows, load_sem.at[0]).wait()
+    for c in order:
         ref = tok_buf.at[tp, chunk(c)]
-        send(ref, tsend.at[0], trecv.at[FAR, c], {"tp": far})
-        send(ref, tsend.at[1], trecv.at[PARTNER, c], {"tp": partner})
-
+        send(ref, tsend.at[0], trecv.at[0, c], {"tp": far})
+
+    own_tok = tok_buf.at[tp]
+    send(own_tok, tsend.at[1], trecv_near.at[0], {"tp": partner})
     forget_load.wait()
     cum_buf[sp] = forget_v[...] * LOG2E
     own_cum = cum_buf.at[sp]
@@ -981,10 +982,10 @@
         sl = pl.ds(n * bw, bw)
         bd_r[sl, sl] = rg_v[n]
         bd_i[sl, sl] = ig_v[n]
-    pltpu.make_async_copy(w_buf, w_buf, load_sem.at[CH]).wait()
+    pltpu.make_async_copy(w_buf, w_buf, load_sem.at[1]).wait()
 
     def tok_wait(src, role, c):
-        arrived(tok_buf.at[src, chunk(c)], trecv.at[role, c])
+        arrived(tok_buf.at[src, chunk(c)], trecv.at[role - 1, c])
 
     def features(side, c):
         first = 2 * side
@@ -998,7 +999,6 @@
         return jnp.sum(v32 * v32, axis=1, keepdims=True)
 
     def near_part(c, slot):
-        tok_wait(partner, PARTNER, c)
         v = features(y, c)
         sq[slot] = squares(v)
         acc[slot] = jnp.dot(v, w_buf[w_rows(y), :], preferred_element_type=F32)
@@ -1035,7 +1035,7 @@
 
     def far_part(i, c, slot):
         tok_wait(far, FAR, c)
-        send(tok_buf.at[far, chunk(c)], tsend.at[2], trecv.at[PFAR, c], {"tp": partner})
+        send(tok_buf.at[far, chunk(c)], tsend.at[2], trecv.at[1, c], {"tp": partner})
         if i + 1 < CH:
             near_part(order[i + 1], 1 - slot)
         tok_wait(pfar, PFAR, c)
@@ -1091,7 +1091,7 @@
         over_y(1)
         c = pl.ds(pl.multiple_of(partner * oc, 128), oc)
         for n, (w, buf) in enumerate(banks):
-            remote(w.at[:, c], buf.at[tp], wsend.at[2], wrecv_own.at[n], {"tp": partner}).start()
+            remote(w.at[:, c], buf.at[tp], wsend.at[2], wrecv_own.at[0], {"tp": partner}).start()
 
     def weight_part(n, role, k):
         t = far if role == FAR else pfar
@@ -1178,6 +1178,7 @@
         else:
             kv_wait(j_bo, c, DIAG)
 
+    arrived(tok_buf.at[partner], trecv_near.at[0])
     near_part(order[0], 0)
     for i, c in enumerate(order):
         far_part(i, c, i % 2)
@@ -1438,10 +1439,10 @@
 
     def send_fox(k):
         ref = br_fox.at[tp, piece(k)]
-        send(ref, fsend.at[0], frecv.at[FAR, k], {"tp": far})
+        send(ref, fsend.at[0], frecv.at[0, k], {"tp": far})
         if k == PC - 1:
-            send(ref, fsend.at[2], frecv.at[PFAR, k], {"tp": pfar})
-        send(ref, fsend.at[1], frecv.at[PARTNER, k], {"tp": partner})
+            send(ref, fsend.at[2], frecv.at[1, k], {"tp": pfar})
+        send(ref, fsend.at[1], frecv_near.at[0], {"tp": partner})
 
     def finish_rows(c):
         r = slice(c * rc, (c + 1) * rc)
@@ -1483,10 +1484,9 @@
         )
 
     def lru_near():
-        for c in own_loads:
-            c.wait()
-        for n in range(2):
-            arrived(banks[n][1].at[partner], wrecv_own.at[n])
+        both = wl_buf.at[pl.ds(0, 2)]
+        pltpu.make_async_copy(both, both, load_sem.at[8]).wait()
+        arrived(both, wrecv_own.at[0])
         arrived(br_lru.at[partner], lrecv.at[PARTNER])
         for c in range(CH):
             oacc[chunk(c), :] = pair_dot(br_lru, wl_buf, y, chunk(c))
@@ -1555,18 +1555,19 @@
         weight_wait(1, role)
 
     def fox_pass(k):
-        arrived(br_fox.at[far, piece(k)], frecv.at[FAR, k])
+        arrived(br_fox.at[far, piece(k)], frecv.at[0, k])
         if k < PC - 1:
-            send(br_fox.at[far, piece(k)], fsend.at[2], frecv.at[PFAR, k], {"tp": partner})
+            send(br_fox.at[far, piece(k)], fsend.at[2], frecv.at[1, k], {"tp": partner})
 
     fox_pass(0)
     for k in range(PC):
         r = piece(k)
         if k + 1 < PC:
             fox_pass(k + 1)
-        arrived(br_fox.at[partner, r], frecv.at[PARTNER, k])
+        if k == 0:
+            arrived(br_fox.at[partner], frecv_near.at[0])
         oacc[r, :] += pair_dot(br_fox, wf_buf, y, r)
-        arrived(br_fox.at[pfar, r], frecv.at[PFAR, k])
+        arrived(br_fox.at[pfar, r], frecv.at[1, k])
         out[r, :] = (oacc[r, :] + pair_dot(br_fox, wf_buf, 1 - y, r)).astype(out.dtype)
 
     for k in range(3):
@@ -1691,9 +1692,10 @@
         V((TP, rows, lw), BF16),
         V((TP, rows, fw), BF16),
         V((rows, oc), F32),
-        dma((CH + 9,)),
+        dma((9,)),
         dma((3,)),
-        dma((3, CH)),
+        dma((1,)),
+        dma((2, CH)),
         dma((1,)),
         dma((1,)),
         dma((1,)),
@@ -1706,12 +1708,13 @@
         dma((1,)),
         dma((3, CH + 1)),
         dma((5,)),
-        dma((2,)),
+        dma((1,)),
         dma((2, 2, X)),
         dma((2,)),
         dma((3,)),
         dma((3,)),
-        dma((3, CH + 1)),
+        dma((1,)),
+        dma((2, CH + 1)),
         dma((1,)),
         dma((2,)),
         dma((2,)),

time: 46.4 us -> 46.2 us (level)
  no operation moved by 1% of the time
where the time goes in v6:
time: 46.2 us; the launch traced here: 45.6 us
  Pallas kernels  44.8 us (97%)
  local copies, waits for them, and re-layouts  0.8 us (2%)
    pallas_call x1, Pallas kernels, block_shards(): pl.pallas_call(functools.partial(block_kernel, SP, TP, X, CH), out_shape=...  44.8 us

profile of v6, /device:TPU:25, one launch (start us, length us, event | category | flops | bytes accessed | tf_op | source)
XLA Modules:
  0.0 45.6 jit_solution(17918156869875449510)
XLA Ops:
  0.0 44.8 %shard_map.136 = bf16[512,512]{1,0:T(8,128)(2,1)S(1)} custom-call(bf16[512,512]{1,0:T(8,128)(2,1)} %tokens.1, bf16[2048,256]{1,0:T(8,128)(2,1)} %lru_in.1, bf16[2048,256]{1,0:T(8,128)(2,1)} %gate_in.1, bf16[2048,256]{1,0:T(8,128)(2,1)} %query_w.1, bf16[2048,256]{1,0:T(8,128)(2,1)} %key_w.1, bf16[2048,256]{1,0:T(8,128)(2,1)} %value_w.1, ...), custom_call_target="tpu_custom_call" | custom-call | tf_op jit(solution)/shard_map/pallas_call | solution.py:1723
  44.8 0.8 %copy.16 = bf16[512,512]{1,0:T(8,128)(2,1)} copy(bf16[512,512]{1,0:T(8,128)(2,1)S(1)} %shard_map.136) | data formatting | bytes 1048576
